TPU v7x, 32 devices: a whole 2x2x4 slice. The times are simulated.
32 devices in a mesh: sp: 8 (over z, x), tp: 4 (over y, core).
Axes of the slice: x: 2, y: 2, z: 4, core: 2. Of those that a mesh axis runs over, the one named last changes fastest.
Arguments:
- tokens: bfloat16 [1024, 2048], P('sp'), may hold values from -6 to 6
- norm_gain: float32 [2048], replicated, may hold values from 0.1 to 1.9
- cotangent: bfloat16 [1024, 2048], P('sp'), may hold values from -8 to 8
- routes: int32 [1024, 2], P('sp'), may hold values from 0 to 3, all different within a row; in each aligned block of 128 rows (0 to 127, 128 to 255, ...) at most 128 rows name the same one
- route_weight: float32 [1024, 2], P('sp'), may hold values from 0.2 to 1
- gate_weight: bfloat16 [8, 2048, 1792], P('sp', None, 'tp'), may hold values from -0.125 to 0.125
- up_weight: bfloat16 [8, 2048, 1792], P('sp', None, 'tp'), may hold values from -0.125 to 0.125
- down_weight: bfloat16 [8, 1792, 2048], P('sp', 'tp'), may hold values from -0.09375 to 0.09375
- scan_input: bfloat16 [1024, 1024], P('sp', 'tp'), may hold values from -6 to 6
- out_gate: bfloat16 [1024, 1024], P('sp', 'tp'), may hold values from -6 to 6
- step_size: float32 [16, 1024], P('tp', 'sp'), may hold values from 0.24 to 4.1
- decay_rate: float32 [16], P('tp'), may hold values from 9.667969e-06 to 0.031
- write_keys: bfloat16 [1024, 256], P('sp', 'tp'), may hold values from -0.75 to 0.75
- read_keys: bfloat16 [1024, 256], P('sp', 'tp'), may hold values from -0.75 to 0.75
- start_state: float32 [8, 16, 64, 64], P('sp', 'tp'), may hold values from -12 to 12
- out_proj: bfloat16 [2048, 1024], P(None, 'tp'), may hold values from -0.1875 to 0.1875
Outputs:
- residual_grad: bfloat16 [1024, 2048], P('sp', 'tp')
- gate_weight_grad: bfloat16 [8, 2048, 1792], P('sp', None, 'tp')
- up_weight_grad: bfloat16 [8, 2048, 1792], P('sp', None, 'tp')
- down_weight_grad: bfloat16 [8, 1792, 2048], P('sp', 'tp')
- out_proj_grad: float32 [2048, 1024], P('sp', 'tp')
- scan_input_grad: bfloat16 [1024, 1024], P('sp', 'tp')
- out_gate_grad: bfloat16 [1024, 1024], P('sp', 'tp')
- write_keys_grad: bfloat16 [1024, 256], P('sp', 'tp')
- read_keys_grad: bfloat16 [1024, 256], P('sp', 'tp')
Inputs may be any that keep to these rules, and one draw needn't show every extreme that they name: Each token names two different experts. Among the tokens of one block of 128 positions at most 128 routes name one expert, and in every draw some expert gets exactly 128 routes from some block.
All inputs are finite; a program needn't handle non-finite values.
Results may differ from a plain program's by a relative error of at most 0.0078.
Values may be sent and summed in bfloat16 or wider, within the bound.
A program may use at most 128 MiB of HBM per device.

v0:
```python
import jax
import jax.numpy as jnp
from jax import lax
from jax.sharding import PartitionSpec as P

D = 2048
HEADS = 16
STATE = 64
GROUPS = 4


EPS = 1e-06
HIGHEST = lax.Precision.HIGHEST


def swapped(value, axis, apart):
    mask = 2**apart
    pairs = [(source, source ^ mask) for source in range(lax.axis_size(axis))]
    return lax.ppermute(value, axis, pairs)


def prefix(part, axis, combine, identity):
    count = lax.axis_size(axis)
    place = lax.axis_index(axis)
    ahead = count - 1 - place
    gathered = jax.tree.map(lambda a: lax.all_gather(a, axis), part)
    state = jax.tree.map(lambda a, e: jnp.zeros_like(a) + jnp.asarray(e, a.dtype), part, identity)

    def one(hop, state):
        source = count - 1 - hop
        return combine(
            state, jax.tree.map(lambda a: lax.dynamic_index_in_dim(a, source, 0, False), gathered)
        )

    return lax.fori_loop(0, ahead, one, state)


def prepare(scan_rows, step_rows, write_rows, read_rows, decay_rates, per_group):
    length = scan_rows.shape[0]
    head_count = step_rows.shape[0]
    logdec = jnp.cumsum(-decay_rates[:, None] * step_rows, axis=1)
    causal = jnp.arange(length)[:, None] >= jnp.arange(length)[None, :]
    spread = jnp.where(causal[None, :, :], logdec[:, :, None] - logdec[:, None, :], -jnp.inf)
    weights = jnp.exp(spread)
    inputs = (
        scan_rows.astype(jnp.float32).reshape(length, head_count, -1)
        * jnp.transpose(step_rows)[:, :, None]
    )
    write_head = jnp.repeat(
        write_rows.astype(jnp.float32).reshape(length, -1, STATE), per_group, axis=1
    )
    read_head = jnp.repeat(
        read_rows.astype(jnp.float32).reshape(length, -1, STATE), per_group, axis=1
    )
    scores = jnp.einsum("thn,shn->hts", read_head, write_head, precision=HIGHEST) * weights
    return (logdec, weights, inputs, write_head, read_head, scores)


def block_forward(
    scan_rows,
    gate_rows,
    step_rows,
    write_rows,
    read_rows,
    decay_rates,
    entry_state,
    mix_grad,
    per_group,
):
    logdec, weights, inputs, write_head, read_head, scores = prepare(
        scan_rows, step_rows, write_rows, read_rows, decay_rates, per_group
    )
    length, head_count = (inputs.shape[0], inputs.shape[1])
    growth = jnp.transpose(jnp.exp(logdec))
    output = jnp.einsum("hts,shp->thp", scores, inputs, precision=HIGHEST)
    output = output + growth[:, :, None] * jnp.einsum(
        "thn,hpn->thp", read_head, entry_state, precision=HIGHEST
    )
    gate_val = gate_rows.astype(jnp.float32).reshape(length, head_count, -1)
    sigmoid_val = jax.nn.sigmoid(gate_val)
    gated = (output * gate_val * sigmoid_val).reshape(length, -1).astype(jnp.bfloat16)
    out_grad = mix_grad.reshape(length, head_count, -1)
    state_grad = out_grad * gate_val * sigmoid_val
    gate_grad = (
        (out_grad * output * sigmoid_val * (1.0 + gate_val * (1.0 - sigmoid_val)))
        .reshape(length, -1)
        .astype(jnp.bfloat16)
    )
    carried = jnp.einsum("th,thp,thn->hpn", growth, state_grad, read_head, precision=HIGHEST)
    return (gated, gate_grad, jnp.exp(logdec[:, -1]), carried, state_grad)


def block_back(
    scan_rows,
    step_rows,
    write_rows,
    read_rows,
    decay_rates,
    entry_state,
    state_grad,
    later_state,
    per_group,
):
    logdec, weights, inputs, write_head, read_head, scores = prepare(
        scan_rows, step_rows, write_rows, read_rows, decay_rates, per_group
    )
    length, head_count = (inputs.shape[0], inputs.shape[1])
    growth = jnp.transpose(jnp.exp(logdec))
    shrink = jnp.transpose(jnp.exp(logdec[:, -1:] - logdec))
    in_grad = jnp.einsum("hts,thp->shp", scores, state_grad, precision=HIGHEST)
    in_grad = in_grad + shrink[:, :, None] * jnp.einsum(
        "shn,hpn->shp", write_head, later_state, precision=HIGHEST
    )
    scan_grad = (
        (in_grad * jnp.transpose(step_rows)[:, :, None]).reshape(length, -1).astype(jnp.bfloat16)
    )
    pair_terms = jnp.einsum("thp,shp->hts", state_grad, inputs, precision=HIGHEST) * weights
    read_grad = jnp.einsum("hts,shn->thn", pair_terms, write_head, precision=HIGHEST)
    read_grad = read_grad + growth[:, :, None] * jnp.einsum(
        "thp,hpn->thn", state_grad, entry_state, precision=HIGHEST
    )
    write_grad = jnp.einsum("hts,thn->shn", pair_terms, read_head, precision=HIGHEST)
    write_grad = write_grad + shrink[:, :, None] * jnp.einsum(
        "shp,hpn->shn", inputs, later_state, precision=HIGHEST
    )
    group_count = head_count // per_group
    read_total = (
        jnp.sum(read_grad.reshape(length, group_count, per_group, -1), axis=2)
        .reshape(length, -1)
        .astype(jnp.bfloat16)
    )
    write_total = (
        jnp.sum(write_grad.reshape(length, group_count, per_group, -1), axis=2)
        .reshape(length, -1)
        .astype(jnp.bfloat16)
    )
    return (scan_grad, write_total, read_total)


def expert_grads(rows_in, rows_cot, gate_mat, up_mat, down_mat):
    contract_rows = (((0,), (0,)), ((), ()))
    contract_cols = (((1,), (1,)), ((), ()))
    gate_pre = jnp.dot(rows_in, gate_mat, preferred_element_type=jnp.float32)
    up_pre = jnp.dot(rows_in, up_mat, preferred_element_type=jnp.float32)
    sigmoid_val = jax.nn.sigmoid(gate_pre)
    active = (gate_pre * sigmoid_val * up_pre).astype(jnp.bfloat16)
    down_grad = lax.dot_general(active, rows_cot, contract_rows, preferred_element_type=jnp.float32)
    act_grad = lax.dot_general(
        rows_cot, down_mat, contract_cols, preferred_element_type=jnp.float32
    )
    gate_pre_grad = (
        act_grad * up_pre * sigmoid_val * (1.0 + gate_pre * (1.0 - sigmoid_val))
    ).astype(jnp.bfloat16)
    up_pre_grad = (act_grad * gate_pre * sigmoid_val).astype(jnp.bfloat16)
    gate_grad = lax.dot_general(
        rows_in, gate_pre_grad, contract_rows, preferred_element_type=jnp.float32
    )
    up_grad = lax.dot_general(
        rows_in, up_pre_grad, contract_rows, preferred_element_type=jnp.float32
    )
    input_grad = lax.dot_general(
        gate_pre_grad, gate_mat, contract_cols, preferred_element_type=jnp.float32
    )
    input_grad = input_grad + lax.dot_general(
        up_pre_grad, up_mat, contract_cols, preferred_element_type=jnp.float32
    )
    return (gate_grad, up_grad, down_grad, input_grad)


def compose(higher, nearer):
    return (nearer[0] * higher[0], nearer[1] + nearer[0][:, None, None] * higher[1])


def shards(
    tokens,
    norm_gain,
    cotangent,
    routes,
    route_weight,
    gate_weight,
    up_weight,
    down_weight,
    scan_input,
    out_gate,
    step_size,
    decay_rate,
    write_keys,
    read_keys,
    start_state,
    out_proj,
):
    sp_count = lax.axis_size("sp")
    tp_count = lax.axis_size("tp")
    tok_rows = tokens.shape[0]
    experts_count = sp_count // 2
    capacity = min(tok_rows, 4 * tok_rows // experts_count)
    quarter = D // tp_count
    hidden = tokens.astype(jnp.float32)
    inverse = lax.rsqrt(jnp.mean(hidden * hidden, axis=1) + EPS)
    normed = (hidden * inverse[:, None] * norm_gain[None, :]).astype(jnp.bfloat16)
    route_flat = routes.reshape(-1)
    member = (route_flat[:, None] == jnp.arange(experts_count, dtype=jnp.int32)[None, :]).astype(
        jnp.int32
    )
    earlier_count = jnp.sum((jnp.cumsum(member, axis=0) - member) * member, axis=1)
    places = (route_flat * capacity + earlier_count).reshape(tok_rows, 2)
    slot_ids = jnp.arange(experts_count * capacity, dtype=jnp.int32)[:, None]
    first_hit = slot_ids == places[None, :, 0]
    second_hit = slot_ids == places[None, :, 1]
    placing = jnp.logical_or(first_hit, second_hit)
    place_matrix = placing.astype(jnp.bfloat16)
    slot_weight = jnp.sum(
        jnp.where(first_hit, route_weight[None, :, 0], 0.0)
        + jnp.where(second_hit, route_weight[None, :, 1], 0.0),
        axis=1,
    )
    send_in = jnp.dot(place_matrix, normed, preferred_element_type=jnp.float32).astype(jnp.bfloat16)
    send_cot = (
        slot_weight[:, None] * jnp.dot(place_matrix, cotangent, preferred_element_type=jnp.float32)
    ).astype(jnp.bfloat16)
    half_cap = capacity // 2
    part_in, part_cot = (
        lax.all_to_all(
            send_in.reshape(sp_count, half_cap, D), "sp", split_axis=0, concat_axis=0, tiled=True
        ),
        lax.all_to_all(
            send_cot.reshape(sp_count, half_cap, D), "sp", split_axis=0, concat_axis=0, tiled=True
        ),
    )
    other_in, other_cot = swapped((part_in, part_cot), "sp", 0)
    lower_bit = lax.axis_index("sp") % 2 == 0
    recv_in = jnp.concatenate(
        [jnp.where(lower_bit, part_in, other_in), jnp.where(lower_bit, other_in, part_in)], axis=1
    )
    recv_cot = jnp.concatenate(
        [jnp.where(lower_bit, part_cot, other_cot), jnp.where(lower_bit, other_cot, part_cot)],
        axis=1,
    )
    rows_in = recv_in.reshape(-1, D)
    rows_cot = recv_cot.reshape(-1, D)
    gate_grad, up_grad, down_grad, input_part = expert_grads(
        rows_in, rows_cot, gate_weight[0], up_weight[0], down_weight[0]
    )
    input_quarter = lax.psum_scatter(input_part, "tp", scatter_dimension=1, tiled=True)
    returned = lax.all_to_all(
        input_quarter.reshape(sp_count, capacity, quarter),
        "sp",
        split_axis=0,
        concat_axis=0,
        tiled=True,
    )
    pair_total = jnp.sum(returned.reshape(experts_count, 2, capacity, quarter), axis=1).reshape(
        -1, quarter
    )
    token_quarter = lax.dot_general(
        placing.astype(jnp.float32), pair_total, (((0,), (0,)), ((), ())), precision=HIGHEST
    )
    normed_grad = lax.all_gather(token_quarter, "tp", axis=1, tiled=True)
    gained = norm_gain[None, :] * normed_grad
    dotted = jnp.sum(hidden * gained, axis=1)
    residual = (
        cotangent.astype(jnp.float32)
        + inverse[:, None] * gained
        - hidden * (inverse**3 * dotted / D)[:, None]
    )
    residual_grad = residual.astype(jnp.bfloat16)
    mix_grad = jnp.dot(residual_grad, out_proj, preferred_element_type=jnp.float32)
    per_group = HEADS // GROUPS
    gated, gate_out_grad, decay_now, carried, state_grad = block_forward(
        scan_input,
        out_gate,
        step_size,
        write_keys,
        read_keys,
        decay_rate,
        start_state[0],
        mix_grad,
        per_group,
    )
    totals, later_state = prefix(
        (decay_now, carried), "sp", compose, (jnp.ones_like(decay_now), jnp.zeros_like(carried))
    )
    scan_grad, write_grad, read_grad = block_back(
        scan_input,
        step_size,
        write_keys,
        read_keys,
        decay_rate,
        start_state[0],
        state_grad,
        later_state,
        per_group,
    )
    out_proj_grad = lax.psum_scatter(
        lax.dot_general(
            residual_grad, gated, (((0,), (0,)), ((), ())), preferred_element_type=jnp.float32
        ),
        "sp",
        scatter_dimension=0,
        tiled=True,
    )
    residual_part = lax.dynamic_slice_in_dim(
        residual_grad, lax.axis_index("tp") * quarter, quarter, 1
    )
    return (
        residual_part,
        gate_grad.astype(jnp.bfloat16)[None],
        up_grad.astype(jnp.bfloat16)[None],
        down_grad.astype(jnp.bfloat16)[None],
        out_proj_grad,
        scan_grad,
        gate_out_grad,
        write_grad,
        read_grad,
    )


def solution(mesh):
    return jax.shard_map(
        shards,
        mesh=mesh,
        in_specs=(
            P("sp", None),
            P(),
            P("sp", None),
            P("sp", None),
            P("sp", None),
            P("sp", None, "tp"),
            P("sp", None, "tp"),
            P("sp", "tp", None),
            P("sp", "tp"),
            P("sp", "tp"),
            P("tp", "sp"),
            P("tp"),
            P("sp", "tp"),
            P("sp", "tp"),
            P("sp", "tp", None, None),
            P(None, "tp"),
        ),
        out_specs=(
            P("sp", "tp"),
            P("sp", None, "tp"),
            P("sp", None, "tp"),
            P("sp", "tp", None),
            P("sp", "tp"),
            P("sp", "tp"),
            P("sp", "tp"),
            P("sp", "tp"),
            P("sp", "tp"),
        ),
        check_vma=False,
    )
```

profile of v0, /device:TPU:0, one launch (start us, length us, event | category | flops | bytes accessed | tf_op | source)
XLA Modules:
  0.0 453.2 jit_solution(3732648020908349817)
XLA Ops:
  8.4 1.2 fusion.24
  9.6 1.2 reduce-window.6
  12.2 3.1 convolution_convert_fusion
  15.3 7.4 %all-to-all-start.1 = ((bf16[8,64,2048]{2,1,0:T(8,128)(2,1)}), bf16[8,64,2048]{2,1,0:T(8,128)(2,1)}, u32[]{:S(2)}, u32[]{:S(2)}) async-start(bf16[8,64,2048]{2,1,0:T(8,128)(2,1)} %bitcast.148), calls=%async_computation.1 | async-start | bytes 4194304 | tf_op jit(solution)/shard_map/all_to_all | solution.py:223
  22.9 2.1 multiply_convert_fusion
  25.0 46.1 %all-to-all-done.1 = bf16[8,64,2048]{2,1,0:T(8,128)(2,1)} async-done(((bf16[8,64,2048]{2,1,0:T(8,128)(2,1)}), bf16[8,64,2048]{2,1,0:T(8,128)(2,1)}, u32[]{:S(2)}, u32[]{:S(2)}) %all-to-all-start.1) | async-done | bytes 2097184 | tf_op jit(solution)/shard_map/all_to_all | solution.py:223
  71.1 4.4 all-to-all-start
  75.7 1.7 collective-permute-start.1
  77.4 46.0 %all-to-all-done = bf16[8,64,2048]{2,1,0:T(8,128)(2,1)} async-done(((bf16[8,64,2048]{2,1,0:T(8,128)(2,1)}), bf16[8,64,2048]{2,1,0:T(8,128)(2,1)}, u32[]{:S(2)}, u32[]{:S(2)}) %all-to-all-start) | async-done | bytes 2097184 | tf_op jit(solution)/shard_map/all_to_all | solution.py:226
  123.3 1.5 collective-permute-start
  124.8 21.8 %collective-permute-done.1 = bf16[8,64,2048]{2,1,0:T(8,128)(2,1)} collective-permute-done((bf16[8,64,2048]{2,1,0:T(8,128)(2,1)}, bf16[8,64,2048]{2,1,0:T(8,128)(2,1)}, u32[]{:S(2)}, u32[]{:S(2)}) %collective-permute-start.1) | collective-permute-done | bytes 2097184 | tf_op jit(solution)/shard_map/ppermute | solution.py:19
  146.6 43.1 %collective-permute-done = bf16[8,64,2048]{2,1,0:T(8,128)(2,1)} collective-permute-done((bf16[8,64,2048]{2,1,0:T(8,128)(2,1)}, bf16[8,64,2048]{2,1,0:T(8,128)(2,1)}, u32[]{:S(2)}, u32[]{:S(2)}) %collective-permute-start) | collective-permute-done | bytes 2097184 | tf_op jit(solution)/shard_map/ppermute | solution.py:19
  189.7 3.7 broadcast_select_fusion.1
  194.0 2.1 fusion.5
  196.9 2.1 fusion.8
  200.3 1.6 copy-done.19
  201.9 2.6 multiply_convert_fusion.2
  204.5 2.4 fusion.3
  206.9 5.9 %convolution_add_fusion = f32[1024,2048]{1,0:T(8,128)} fusion(f32[1024,2048]{1,0:T(8,128)S(1)} %fusion.3, bf16[1024,448]{0,1:T(8,128)(2,1)S(1)} %get-tuple-element.164, bf16[1,2048,448]{1,2,0:T(8,128)(2,1)S(1)} %copy-done.9), kind=kOutput, calls=%fused_computation.5 | convolution fusion | flops 1881145344 | bytes 19529728 | tf_op jit(solution)/shard_map/dot_general | solution.py:164
  212.8 71.4 %reduce-scatter.3.cloned.1.call-done = f32[1024,512]{1,0:T(8,128)} async-done(((f32[1024,2048]{1,0:T(8,128)}), f32[1024,512]{1,0:T(8,128)}) %reduce-scatter.3.cloned.1.call-update) | async-done | bytes 2097168 | tf_op jit(solution)/shard_map/reduce_scatter | solution.py:244
  284.2 5.6 %all-to-all-start.2 = ((f32[8,128,512]{2,1,0:T(8,128)}), f32[8,128,512]{2,1,0:T(8,128)}, u32[]{:S(2)}, u32[]{:S(2)}) async-start(f32[8,128,512]{2,1,0:T(8,128)} %bitcast.157), calls=%async_computation.3 | async-start | bytes 4194304 | tf_op jit(solution)/shard_map/all_to_all | solution.py:245
  290.2 47.8 %all-to-all-done.2 = f32[8,128,512]{2,1,0:T(8,128)} async-done(((f32[8,128,512]{2,1,0:T(8,128)}), f32[8,128,512]{2,1,0:T(8,128)}, u32[]{:S(2)}, u32[]{:S(2)}) %all-to-all-start.2) | async-done | bytes 2097184 | tf_op jit(solution)/shard_map/all_to_all | solution.py:245
  338.0 1.9 bitcast_reduce_fusion
  339.9 1.3 fusion.35
  343.4 19.5 %all-reduce = f32[32]{0:T(128)S(1)} all-reduce(f32[32]{0:T(128)S(1)} %dynamic-update-slice), channel_id=3, replica_groups=mesh['sp'=8,'tp'=4] {'sp'}, use_global_device_ids=true, to_apply=%add | all-reduce | flops 32 | bytes 256
  364.2 5.8 %fusion.2 = bf16[1,2048,448]{1,2,0:T(8,128)(2,1)} fusion(bf16[1024,448]{0,1:T(8,128)(2,1)} %copy-done.8, bf16[1024,2048]{1,0:T(8,128)(2,1)} %bitcast.152), kind=kOutput, calls=%fused_computation.12 | convolution fusion | flops 1879965696 | bytes 6946816 | tf_op jit(solution)/shard_map/dot_general | solution.py:158
  370.0 1.6 fusion.27
  373.3 1.8 fusion.69
  375.2 5.6 %fusion.1 = bf16[1,2048,448]{1,2,0:T(8,128)(2,1)} fusion(bf16[1024,448]{0,1:T(8,128)(2,1)S(1)} %copy-done.23, bf16[1024,2048]{1,0:T(8,128)(2,1)} %bitcast.153), kind=kOutput, calls=%fused_computation.11 | convolution fusion | flops 1879965696 | bytes 6946816 | tf_op jit(solution)/shard_map/dot_general | solution.py:155
  380.8 3.4 fusion
  385.3 34.7 %all-gather = f32[32,64,64]{2,1,0:T(8,128)S(1)} all-gather(f32[4,64,64]{2,1,0:T(8,128)S(1)} %fusion.41), channel_id=2, replica_groups=mesh['sp'=8,'tp'=4] {'sp'}, dimensions={0}, use_global_device_ids=true | all-gather | bytes 589824 | tf_op jit(solution)/shard_map/all_gather | solution.py:26
  426.5 20.1 %reduce-scatter.5.cloned.1.call-done = f32[256,256]{1,0:T(8,128)} async-done(((f32[2048,256]{1,0:T(8,128)}), f32[256,256]{1,0:T(8,128)}) %reduce-scatter.5.cloned.1.call-update) | async-done | bytes 262160 | tf_op jit(solution)/shard_map/reduce_scatter | solution.py:294
  (129 shorter events, 18.5 us)
Async XLA Ops:
  7.2 186.9 %copy-start = (bf16[1,2048,448]{1,2,0:T(8,128)(2,1)S(1)}, bf16[1,2048,448]{1,2,0:T(8,128)(2,1)}, u32[]{:S(2)}) copy-start(bf16[1,2048,448]{1,2,0:T(8,128)(2,1)} %param.23) | copy-start | bytes 5505028
  15.3 7.4 %copy-start.18 = (f32[128,2]{0,1:T(2,128)S(1)}, f32[128,2]{0,1:T(2,128)}, u32[]{:S(2)}) copy-start(f32[128,2]{0,1:T(2,128)} %param.22) | copy-start | bytes 3076
  15.3 7.6 %copy-start.7 = (bf16[128,2048]{1,0:T(8,128)(2,1)S(1)}, bf16[128,2048]{1,0:T(8,128)(2,1)}, u32[]{:S(2)}) copy-start(bf16[128,2048]{1,0:T(8,128)(2,1)} %param.20) | copy-start | bytes 1572868
  15.3 55.8 %all-to-all-start.1 = ((bf16[8,64,2048]{2,1,0:T(8,128)(2,1)}), bf16[8,64,2048]{2,1,0:T(8,128)(2,1)}, u32[]{:S(2)}, u32[]{:S(2)}) async-start(bf16[8,64,2048]{2,1,0:T(8,128)(2,1)} %bitcast.148), calls=%async_computation.1 | async-start | bytes 4194304 | tf_op jit(solution)/shard_map/all_to_all | solution.py:223
  71.1 52.2 %all-to-all-start = ((bf16[8,64,2048]{2,1,0:T(8,128)(2,1)}), bf16[8,64,2048]{2,1,0:T(8,128)(2,1)}, u32[]{:S(2)}, u32[]{:S(2)}) async-start(bf16[8,64,2048]{2,1,0:T(8,128)(2,1)} %bitcast.147), calls=%async_computation | async-start | bytes 4194304 | tf_op jit(solution)/shard_map/all_to_all | solution.py:226
  75.5 208.8 %reduce-scatter.3.cloned.1.call-start = ((), (), s32[]{:S(2)}) async-start(), calls=%async_computation.5 | async-start | bytes 10485760 | tf_op jit(solution)/shard_map/reduce_scatter | solution.py:244
  75.7 70.9 %collective-permute-start.1 = (bf16[8,64,2048]{2,1,0:T(8,128)(2,1)}, bf16[8,64,2048]{2,1,0:T(8,128)(2,1)}, u32[]{:S(2)}, u32[]{:S(2)}) collective-permute-start(bf16[8,64,2048]{2,1,0:T(8,128)(2,1)} %all-to-all-done.1), channel_id=1, source_target_pairs={{0,4},{4,0},{8,12},{12,8},{16,20},{20,16},{24,28},{28,24},{1,5},{5... | collective-permute-start | bytes 6291464 | tf_op jit(solution)/shard_map/ppermute | solution.py:19
  123.3 66.4 %collective-permute-start = (bf16[8,64,2048]{2,1,0:T(8,128)(2,1)}, bf16[8,64,2048]{2,1,0:T(8,128)(2,1)}, u32[]{:S(2)}, u32[]{:S(2)}) collective-permute-start(bf16[8,64,2048]{2,1,0:T(8,128)(2,1)} %all-to-all-done), channel_id=1, source_target_pairs={{0,4},{4,0},{8,12},{12,8},{16,20},{20,16},{24,28},{28,24},{1,5},{5... | collective-permute-start | bytes 6291464 | tf_op jit(solution)/shard_map/ppermute | solution.py:19
  194.0 2.1 copy-start.4
  194.0 2.9 copy-start.9
  196.9 2.7 copy-start.24
  199.0 2.9 copy-start.19
  199.6 4.8 %copy-start.5 = (bf16[8,128,2048]{2,1,0:T(8,128)(2,1)}, bf16[8,128,2048]{2,1,0:T(8,128)(2,1)S(1)}, u32[]{:S(2)}) copy-start(bf16[8,128,2048]{2,1,0:T(8,128)(2,1)S(1)} %pad_maximum_fusion) | copy-start | bytes 12582916
  204.5 2.4 copy-start.22
  204.5 2.4 copy-start.8
  284.2 5.9 %copy-start.20 = (f32[4]{0:T(128)S(1)}, f32[4]{0:T(128)}, u32[]{:S(2)}) copy-start(f32[4]{0:T(128)} %param.29) | copy-start | bytes 52
  284.2 53.8 %all-to-all-start.2 = ((f32[8,128,512]{2,1,0:T(8,128)}), f32[8,128,512]{2,1,0:T(8,128)}, u32[]{:S(2)}, u32[]{:S(2)}) async-start(f32[8,128,512]{2,1,0:T(8,128)} %bitcast.157), calls=%async_computation.3 | async-start | bytes 4194304 | tf_op jit(solution)/shard_map/all_to_all | solution.py:245
  289.9 80.2 %all-gather.4.cloned.1.call-start = ((), (), s32[]{:S(2)}) async-start(), calls=%async_computation.6 | async-start | bytes 1310720 | tf_op jit(solution)/shard_map/all_gather | solution.py:258
  290.1 51.2 %copy-start.15 = (f32[4,128]{1,0:T(4,128)S(1)}, f32[4,128]{1,0:T(4,128)}, u32[]{:S(2)}) copy-start(f32[4,128]{1,0:T(4,128)} %param.28) | copy-start | bytes 6148
  290.2 51.2 %copy-start.21 = (u32[32]{0:T(128)S(1)}, u32[32]{0:T(128)}, u32[]{:S(2)}) copy-start(u32[32]{0:T(128)} %constant.92) | copy-start | bytes 388
  290.2 72.7 %copy-start.16 = (bf16[128,64]{0,1:T(8,128)(2,1)S(1)}, bf16[128,64]{0,1:T(8,128)(2,1)}, u32[]{:S(2)}) copy-start(bf16[128,64]{0,1:T(8,128)(2,1)} %param.31) | copy-start | bytes 49156
  290.2 72.7 %copy-start.17 = (bf16[128,64]{0,1:T(8,128)(2,1)S(1)}, bf16[128,64]{0,1:T(8,128)(2,1)}, u32[]{:S(2)}) copy-start(bf16[128,64]{0,1:T(8,128)(2,1)} %param.30) | copy-start | bytes 49156
  290.2 72.8 %copy-start.13 = (bf16[128,256]{1,0:T(8,128)(2,1)S(1)}, bf16[128,256]{1,0:T(8,128)(2,1)}, u32[]{:S(2)}) copy-start(bf16[128,256]{1,0:T(8,128)(2,1)} %param.26) | copy-start | bytes 196612
  290.2 72.9 %copy-start.14 = (bf16[128,256]{1,0:T(8,128)(2,1)S(1)}, bf16[128,256]{1,0:T(8,128)(2,1)}, u32[]{:S(2)}) copy-start(bf16[128,256]{1,0:T(8,128)(2,1)} %param.27) | copy-start | bytes 196612
  290.2 73.1 %copy-start.11 = (f32[1,4,64,64]{3,2,1,0:T(8,128)S(1)}, f32[1,4,64,64]{3,2,1,0:T(8,128)}, u32[]{:S(2)}) copy-start(f32[1,4,64,64]{3,2,1,0:T(8,128)} %param.32) | copy-start | bytes 196612
  341.2 105.4 %reduce-scatter.5.cloned.1.call-start = ((), (), s32[]{:S(2)}) async-start(), calls=%async_computation.7 | async-start | bytes 2359296 | tf_op jit(solution)/shard_map/reduce_scatter | solution.py:294
  364.2 5.8 %copy-start.2 = (bf16[128,2048]{1,0:T(8,128)(2,1)S(1)}, bf16[128,2048]{1,0:T(8,128)(2,1)}, u32[]{:S(2)}) copy-start(bf16[128,2048]{1,0:T(8,128)(2,1)} %param.18) | copy-start | bytes 1572868
  364.2 5.8 %copy-start.12 = (f32[2048]{0:T(1024)S(1)}, f32[2048]{0:T(1024)}, u32[]{:S(2)}) copy-start(f32[2048]{0:T(1024)} %param.19) | copy-start | bytes 24580
  375.1 5.7 %copy-start.6 = (bf16[8,128,2048]{2,1,0:T(8,128)(2,1)S(1)}, bf16[8,128,2048]{2,1,0:T(8,128)(2,1)}, u32[]{:S(2)}) copy-start(bf16[8,128,2048]{2,1,0:T(8,128)(2,1)} %copy-done.5) | copy-start | bytes 12582916
  375.1 5.7 %copy-start.25 = (f32[1024,448]{0,1:T(8,128)S(1)}, f32[1024,448]{0,1:T(8,128)}, u32[]{:S(2)}) copy-start(f32[1024,448]{0,1:T(8,128)} %copy-done.24) | copy-start | bytes 5505028
  375.1 5.7 %copy-start.27 = (f32[1024,448]{0,1:T(8,128)S(1)}, f32[1024,448]{0,1:T(8,128)}, u32[]{:S(2)}) copy-start(f32[1024,448]{0,1:T(8,128)} %copy-done.26) | copy-start | bytes 5505028
  420.9 25.8 %copy-start.1 = (bf16[1,2048,448]{1,2,0:T(8,128)(2,1)S(1)}, bf16[1,2048,448]{1,2,0:T(8,128)(2,1)}, u32[]{:S(2)}) copy-start(bf16[1,2048,448]{1,2,0:T(8,128)(2,1)} %param.23) | copy-start | bytes 5505028
  (4 other events, 6.8 us)
Sparse Core Ops, SparseCore 0:
  212.9 71.2 reduce-scatter.2
  341.4 14.8 all-gather.3
  375.2 71.3 reduce-scatter.4
where the time goes:
time: 454 us; the launch traced here: 453 us
  waiting for transfers between devices  296 us (65%)
  blocking collectives  54.2 us (12%)
  matrix products  44.7 us (10%)
  starting transfers between devices  21 us (5%)
  between operations  15 us (3%)
  other arithmetic  13.3 us (3%)
  local copies, waits for them, and re-layouts  8.36 us (2%)
    reduce_scatter x1, waiting for transfers between devices, shards(): lax.psum_scatter(input_part, 'tp', scatter_dimension=1, tiled=True)  71.4 us
    ppermute x2, waiting for transfers between devices, swapped(): return lax.ppermute(value, axis, pairs)  65 us
    all_to_all x1, waiting for transfers between devices, shards(): lax.all_to_all(input_quarter.reshape(sp_count, capacity, quarter), 'sp',...  47.8 us
    all_to_all x1, waiting for transfers between devices, shards(): lax.all_to_all(send_in.reshape(sp_count, half_cap, D), 'sp', split_axis=0...  46.1 us
    all_to_all x1, waiting for transfers between devices, shards(): lax.all_to_all(send_cot.reshape(sp_count, half_cap, D), 'sp', split_axis=...  46 us
    all_gather x1, blocking collectives, prefix(): gathered = jax.tree.map(lambda a: lax.all_gather(a, axis), part)  34.7 us
    reduce_scatter x1, waiting for transfers between devices, shards(): lax.psum_scatter(lax.dot_general(residual_grad, gated, (((0,), (0,)), (()...  20.1 us
    unnamed x1, blocking collectives  19.5 us
  transfers between devices with their start and end apart: 8, of which 7 were waited for; matrix products, arithmetic and copies ran while one was open for 6% of the time, Pallas kernels for 0%

commit v1 on v0

--- a/solution.py
+++ b/solution.py
@@ -1,6 +1,10 @@
+import functools
+
 import jax
 import jax.numpy as jnp
 from jax import lax
+from jax.experimental import pallas as pl
+from jax.experimental.pallas import tpu as pltpu
 from jax.sharding import PartitionSpec as P
 
 D = 2048
@@ -169,6 +173,464 @@
 
 def compose(higher, nearer):
     return (nearer[0] * higher[0], nearer[1] + nearer[0][:, None, None] * higher[1])
+
+
+MESH = pl.DeviceIdType.MESH
+
+
+def remote(src, dst, send, recv, device):
+    return pltpu.make_async_remote_copy(
+        src_ref=src,
+        dst_ref=dst,
+        send_sem=send,
+        recv_sem=recv,
+        device_id=device,
+        device_id_type=MESH,
+    )
+
+
+def greet(devices):
+    barrier = pltpu.get_barrier_semaphore()
+    for device in devices:
+        pl.semaphore_signal(barrier, inc=1, device_id=device, device_id_type=MESH)
+    pl.semaphore_wait(barrier, len(devices))
+
+
+def gather_kernel(
+    nz, a_ref, b_ref, w_ref, oa_ref, ob_ref, ow_ref, own_sem, z_send, z_recv, x_sem, y_sem, c_sem, d_sem, w_sem
+):
+    rows = a_ref.shape[0]
+    part = rows // 4
+    sp, tp = lax.axis_index("sp"), lax.axis_index("tp")
+    z, x, y, c = sp // 2, sp % 2, tp // 2, tp % 2
+    count = 2 * nz
+    over_x = (z * 2 + 1 - x, tp)
+    over_y = (sp, (1 - y) * 2 + c)
+    over_c = (sp, y * 2 + 1 - c)
+    peers = [((sp + k) % count, tp) for k in range(1, count)]
+    greet(peers + [over_y, over_c])
+
+    def span(core, row, whole):
+        if whole:
+            return core * (2 * part), 2 * part
+        return core * (2 * part) + row * part, part
+
+    def copies(block, piece, send, recv, device, own=False):
+        start, size = piece
+        made = []
+        for k, (src, dst) in enumerate(((a_ref, oa_ref), (b_ref, ob_ref))):
+            at = pl.ds(pl.multiple_of(block * rows + start, part), size)
+            source = src.at[pl.ds(pl.multiple_of(start, part), size)] if own else dst.at[at]
+            made.append(remote(source, dst.at[at], send.at[k, block], recv.at[k, block], device))
+        return made
+
+    def go(made):
+        for copy in made:
+            copy.start()
+
+    def arrived(made):
+        for copy in made:
+            copy.wait_recv()
+
+    def sent(made):
+        for copy in made:
+            copy.wait_send()
+
+    mine_half = span(c, y, True)
+    mine_part = span(c, y, False)
+    y_part = span(c, 1 - y, False)
+    for k in range(1, count):
+        other = ((sp + k) % count, tp)
+        remote(w_ref, ow_ref.at[sp], w_sem.at[0, k], w_sem.at[1, k], other).start()
+    steps = []
+
+    def send_if(condition, make):
+        if condition is None:
+            go(make())
+        else:
+            @pl.when(condition)
+            def _():
+                go(make())
+        steps.append((condition, make))
+
+    up = (jnp.minimum(z + 1, nz - 1) * 2 + x, tp)
+    down = (jnp.maximum(z - 1, 0) * 2 + x, tp)
+    own = z * 2 + x
+    send_if(z < nz - 1, lambda: copies(own, mine_half, z_send.at[0], z_recv, up, True))
+    send_if(z > 0, lambda: copies(own, mine_half, z_send.at[1], z_recv, down, True))
+    send_if(None, lambda: copies(own, mine_half, x_sem.at[0], x_sem.at[1], over_x, True))
+    locals_ = [
+        pltpu.make_async_copy(src, dst.at[pl.ds(pl.multiple_of(own * rows, rows), rows)], own_sem.at[k])
+        for k, (src, dst) in enumerate(((a_ref, oa_ref), (b_ref, ob_ref)))
+    ]
+    locals_.append(pltpu.make_async_copy(w_ref, ow_ref.at[sp], own_sem.at[2]))
+    go(locals_)
+
+    def sides(step):
+        if step == 0:
+            return [(None, z, 0)]
+        return [(z - step >= 0, z - step, 0), (z + step <= nz - 1, z + step, 1)]
+
+    def guarded(condition, work):
+        if condition is None:
+            work()
+        else:
+            pl.when(condition)(work)
+
+    def from_z(step):
+        for condition, at, way in sides(step):
+            block = at * 2 + x
+            piece = mine_half if step == 1 else mine_part
+            guarded(condition, lambda: arrived(copies(block, piece, z_send.at[way], z_recv, up)))
+            onward = jnp.logical_and(condition, z < nz - 1 if way == 0 else z > 0)
+            target = up if way == 0 else down
+            send_if(
+                onward,
+                lambda block=block, way=way, target=target: copies(
+                    block, mine_part, z_send.at[way], z_recv, target
+                ),
+            )
+            send_if(
+                condition,
+                lambda block=block: copies(block, mine_part, x_sem.at[0], x_sem.at[1], over_x),
+            )
+            if step >= 2:
+                send_if(
+                    condition,
+                    lambda block=block: copies(block, mine_part, y_sem.at[0], y_sem.at[1], over_y),
+                )
+            send_if(
+                condition,
+                lambda block=block, piece=piece: copies(
+                    block, piece, c_sem.at[0], c_sem.at[1], over_c
+                ),
+            )
+
+    def from_x(step):
+        for condition, at, way in sides(step):
+            block = at * 2 + 1 - x
+            piece = mine_half if step == 0 else mine_part
+            guarded(
+                condition,
+                lambda: arrived(copies(block, piece, x_sem.at[0], x_sem.at[1], over_x)),
+            )
+            if step >= 1:
+                send_if(
+                    condition,
+                    lambda block=block: copies(block, mine_part, y_sem.at[0], y_sem.at[1], over_y),
+                )
+            send_if(
+                condition,
+                lambda block=block, piece=piece: copies(
+                    block, piece, c_sem.at[0], c_sem.at[1], over_c
+                ),
+            )
+
+    def from_y(step, column):
+        for condition, at, way in sides(step):
+            block = at * 2 + column
+            guarded(
+                condition,
+                lambda: arrived(copies(block, y_part, y_sem.at[0], y_sem.at[1], over_y)),
+            )
+            send_if(
+                condition,
+                lambda block=block: copies(block, y_part, d_sem.at[0], d_sem.at[1], over_c),
+            )
+
+    for step in range(nz + 2):
+        if 1 <= step < nz:
+            from_z(step)
+        if 0 <= step - 1 < nz:
+            from_x(step - 1)
+        if 2 <= step - 1 < nz:
+            from_y(step - 1, x)
+        if 1 <= step - 2 < nz:
+            from_y(step - 2, 1 - x)
+
+    for step in range(nz):
+        for condition, at, way in sides(step):
+            for column, first, then in ((x, 1, 2), (1 - x, 0, 1)):
+                block = at * 2 + column
+                if step >= first:
+                    piece = span(1 - c, y, step == first)
+                    guarded(
+                        condition,
+                        lambda: arrived(copies(block, piece, c_sem.at[0], c_sem.at[1], over_c)),
+                    )
+                if step >= then:
+                    piece = span(1 - c, 1 - y, False)
+                    guarded(
+                        condition,
+                        lambda: arrived(copies(block, piece, d_sem.at[0], d_sem.at[1], over_c)),
+                    )
+    for k in range(1, count):
+        source = (sp + count - k) % count
+        remote(w_ref, ow_ref.at[source], w_sem.at[0, k], w_sem.at[1, k], over_x).wait_recv()
+    for k in range(1, count):
+        remote(w_ref, ow_ref.at[sp], w_sem.at[0, k], w_sem.at[1, k], over_x).wait_send()
+    for condition, make in steps:
+        guarded(condition, lambda: sent(make()))
+    for copy in locals_:
+        copy.wait()
+
+
+def gather_rows(nz, first, second, weights):
+    count = 2 * nz
+    rows, width = first.shape
+    dma = pltpu.SemaphoreType.DMA
+    whole = jax.ShapeDtypeStruct((count * rows, width), first.dtype)
+    return pl.pallas_call(
+        functools.partial(gather_kernel, nz),
+        out_shape=(whole, whole, jax.ShapeDtypeStruct((count,) + weights.shape, weights.dtype)),
+        in_specs=[pl.BlockSpec(memory_space=pltpu.VMEM)] * 3,
+        out_specs=(pl.BlockSpec(memory_space=pl.ANY),) * 3,
+        scratch_shapes=[
+            dma((3,)),
+            dma((2, 2, count)),
+            dma((2, count)),
+            dma((2, 2, count)),
+            dma((2, 2, count)),
+            dma((2, 2, count)),
+            dma((2, 2, count)),
+            dma((2, count)),
+        ],
+        compiler_params=pltpu.CompilerParams(collective_id=0, has_side_effects=True),
+        name="gather_rows",
+    )(first, second, weights)
+
+
+def total_kernel(
+    nz, p_ref, o_ref, rc, s1, ra, rb, sa, sb, r2, s3, rz, full, c_sem, m_sem, n_sem, z_sem, g_sem
+):
+    width = p_ref.shape[1]
+    half, quarter = width // 2, width // 4
+    rows = p_ref.shape[0] // (2 * nz)
+    sp, tp = lax.axis_index("sp"), lax.axis_index("tp")
+    z, x, y, c = sp // 2, sp % 2, tp // 2, tp % 2
+    over_x = (z * 2 + 1 - x, tp)
+    over_y = (sp, (1 - y) * 2 + c)
+    over_c = (sp, y * 2 + 1 - c)
+    f32, bf16 = jnp.float32, jnp.bfloat16
+    greet([(((z + k) % nz) * 2 + x, tp) for k in range(1, nz)] + [over_x, over_y, over_c])
+
+    def lanes(index, size):
+        return pl.ds(pl.multiple_of(index * size, size), size)
+
+    def plane(i):
+        return (z + 1 + i) % nz
+
+    made = []
+
+    def core_copy(i):
+        at = lanes(plane(i), 2 * rows)
+        return remote(
+            p_ref.at[at, lanes(1 - c, half)], rc.at[at], c_sem.at[0, i], c_sem.at[1, i], over_c
+        )
+
+    for i in range(nz):
+        copy = core_copy(i)
+        copy.start()
+        made.append(copy)
+    firsts, seconds = [], []
+    for i in range(nz):
+        made[i].wait_recv()
+        at = lanes(plane(i), 2 * rows)
+        s1[at] = (p_ref[at, lanes(c, half)].astype(f32) + rc[at].astype(f32)).astype(bf16)
+        if i % 2 == 0:
+            copy = remote(
+                s1.at[at, lanes(1 - y, quarter)],
+                ra.at[i // 2],
+                m_sem.at[0, i],
+                m_sem.at[1, i],
+                over_y,
+            )
+        else:
+            copy = remote(
+                s1.at[lanes(plane(i) * 2 + 1 - x, rows)],
+                rb.at[i // 2],
+                m_sem.at[0, i],
+                m_sem.at[1, i],
+                over_x,
+            )
+        copy.start()
+        firsts.append(copy)
+    for i in range(nz):
+        firsts[i].wait_recv()
+        k = i // 2
+        if i % 2 == 0:
+            at = lanes(plane(i), 2 * rows)
+            sa[k] = (s1[at, lanes(y, quarter)].astype(f32) + ra[k].astype(f32)).astype(bf16)
+            copy = remote(
+                sa.at[k, lanes(1 - x, rows)], r2.at[i], n_sem.at[0, i], n_sem.at[1, i], over_x
+            )
+        else:
+            at = lanes(plane(i) * 2 + x, rows)
+            sb[k] = (s1[at].astype(f32) + rb[k].astype(f32)).astype(bf16)
+            copy = remote(
+                sb.at[k, :, lanes(1 - y, quarter)],
+                r2.at[i],
+                n_sem.at[0, i],
+                n_sem.at[1, i],
+                over_y,
+            )
+        copy.start()
+        seconds.append(copy)
+    along = []
+    total = None
+    for i in range(nz):
+        seconds[i].wait_recv()
+        k = i // 2
+        held = sa[k, lanes(x, rows)] if i % 2 == 0 else sb[k, :, lanes(y, quarter)]
+        value = held.astype(f32) + r2[i].astype(f32)
+        if i < nz - 1:
+            s3[i] = value.astype(bf16)
+            copy = remote(
+                s3.at[i], rz.at[i], z_sem.at[0, i], z_sem.at[1, i], (plane(i) * 2 + x, tp)
+            )
+            copy.start()
+            along.append(copy)
+        else:
+            total = value
+    for i in range(nz - 1):
+        along[i].wait_recv()
+        total = total + rz[i].astype(f32)
+    mine = c * 2 + y
+    theirs = c * 2 + 1 - y
+    full[:, lanes(mine, quarter)] = total.astype(bf16)
+    own = full.at[:, lanes(mine, quarter)]
+    to_y = remote(own, own, g_sem.at[0, 0], g_sem.at[1, 0], over_y)
+    to_c = remote(own, own, g_sem.at[0, 1], g_sem.at[1, 1], over_c)
+    to_y.start()
+    to_c.start()
+    to_y.wait_recv()
+    got = full.at[:, lanes(theirs, quarter)]
+    onward = remote(got, got, g_sem.at[0, 2], g_sem.at[1, 2], over_c)
+    onward.start()
+    to_c.wait_recv()
+    onward.wait_recv()
+    o_ref[...] = full[...]
+    for copy in made + firsts + seconds + along + [to_y, to_c, onward]:
+        copy.wait_send()
+
+
+def total_rows(nz, parts):
+    count = 2 * nz
+    rows, width = parts.shape[0] // count, parts.shape[1]
+    half, quarter = width // 2, width // 4
+    evens, odds = (nz + 1) // 2, max(nz // 2, 1)
+    dma = pltpu.SemaphoreType.DMA
+    vmem = functools.partial(pltpu.VMEM, dtype=jnp.bfloat16)
+    return pl.pallas_call(
+        functools.partial(total_kernel, nz),
+        out_shape=jax.ShapeDtypeStruct((rows, width), jnp.bfloat16),
+        in_specs=[pl.BlockSpec(memory_space=pltpu.VMEM)],
+        out_specs=pl.BlockSpec(memory_space=pltpu.VMEM),
+        scratch_shapes=[
+            vmem((count * rows, half)),
+            vmem((count * rows, half)),
+            vmem((evens, 2 * rows, quarter)),
+            vmem((odds, rows, half)),
+            vmem((evens, 2 * rows, quarter)),
+            vmem((odds, rows, half)),
+            vmem((nz, rows, quarter)),
+            vmem((nz, rows, quarter)),
+            vmem((nz, rows, quarter)),
+            vmem((rows, width)),
+            dma((2, nz)),
+            dma((2, nz)),
+            dma((2, nz)),
+            dma((2, nz)),
+            dma((2, 3)),
+        ],
+        compiler_params=pltpu.CompilerParams(collective_id=1, has_side_effects=True),
+        name="total_rows",
+    )(parts)
+
+
+def dense_grads(normed, cotangent, routes, route_weight, gate_mat, up_mat, down_mat):
+    sp_count = lax.axis_size("sp")
+    experts_count = sp_count // 2
+    nz = sp_count // 2
+    names = jnp.arange(experts_count, dtype=jnp.int32)[:, None]
+    table = jnp.where(routes[None, :, 0] == names, route_weight[None, :, 0], 0.0)
+    table = table + jnp.where(routes[None, :, 1] == names, route_weight[None, :, 1], 0.0)
+    rows_in, cot_all, tables = gather_rows(nz, normed, cotangent, table)
+    weight_all = lax.dynamic_index_in_dim(tables, lax.axis_index("sp") // 2, 1, False).reshape(-1)
+    rows_cot = (weight_all[:, None] * cot_all.astype(jnp.float32)).astype(jnp.bfloat16)
+    gate_grad, up_grad, down_grad, input_part = expert_grads(
+        rows_in, rows_cot, gate_mat, up_mat, down_mat
+    )
+    normed_grad = total_rows(nz, input_part.astype(jnp.bfloat16)).astype(jnp.float32)
+    return gate_grad, up_grad, down_grad, normed_grad
+
+
+def routed_grads(normed, cotangent, routes, route_weight, gate_mat, up_mat, down_mat):
+    sp_count = lax.axis_size("sp")
+    tp_count = lax.axis_size("tp")
+    tok_rows = normed.shape[0]
+    experts_count = sp_count // 2
+    capacity = min(tok_rows, 4 * tok_rows // experts_count)
+    quarter = D // tp_count
+    route_flat = routes.reshape(-1)
+    member = (route_flat[:, None] == jnp.arange(experts_count, dtype=jnp.int32)[None, :]).astype(
+        jnp.int32
+    )
+    earlier_count = jnp.sum((jnp.cumsum(member, axis=0) - member) * member, axis=1)
+    places = (route_flat * capacity + earlier_count).reshape(tok_rows, 2)
+    slot_ids = jnp.arange(experts_count * capacity, dtype=jnp.int32)[:, None]
+    first_hit = slot_ids == places[None, :, 0]
+    second_hit = slot_ids == places[None, :, 1]
+    placing = jnp.logical_or(first_hit, second_hit)
+    place_matrix = placing.astype(jnp.bfloat16)
+    slot_weight = jnp.sum(
+        jnp.where(first_hit, route_weight[None, :, 0], 0.0)
+        + jnp.where(second_hit, route_weight[None, :, 1], 0.0),
+        axis=1,
+    )
+    send_in = jnp.dot(place_matrix, normed, preferred_element_type=jnp.float32).astype(jnp.bfloat16)
+    send_cot = (
+        slot_weight[:, None] * jnp.dot(place_matrix, cotangent, preferred_element_type=jnp.float32)
+    ).astype(jnp.bfloat16)
+    half_cap = capacity // 2
+    part_in, part_cot = (
+        lax.all_to_all(
+            send_in.reshape(sp_count, half_cap, D), "sp", split_axis=0, concat_axis=0, tiled=True
+        ),
+        lax.all_to_all(
+            send_cot.reshape(sp_count, half_cap, D), "sp", split_axis=0, concat_axis=0, tiled=True
+        ),
+    )
+    other_in, other_cot = swapped((part_in, part_cot), "sp", 0)
+    lower_bit = lax.axis_index("sp") % 2 == 0
+    recv_in = jnp.concatenate(
+        [jnp.where(lower_bit, part_in, other_in), jnp.where(lower_bit, other_in, part_in)], axis=1
+    )
+    recv_cot = jnp.concatenate(
+        [jnp.where(lower_bit, part_cot, other_cot), jnp.where(lower_bit, other_cot, part_cot)],
+        axis=1,
+    )
+    rows_in = recv_in.reshape(-1, D)
+    rows_cot = recv_cot.reshape(-1, D)
+    gate_grad, up_grad, down_grad, input_part = expert_grads(
+        rows_in, rows_cot, gate_mat, up_mat, down_mat
+    )
+    input_quarter = lax.psum_scatter(input_part, "tp", scatter_dimension=1, tiled=True)
+    returned = lax.all_to_all(
+        input_quarter.reshape(sp_count, capacity, quarter),
+        "sp",
+        split_axis=0,
+        concat_axis=0,
+        tiled=True,
+    )
+    pair_total = jnp.sum(returned.reshape(experts_count, 2, capacity, quarter), axis=1).reshape(
+        -1, quarter
+    )
+    token_quarter = lax.dot_general(
+        placing.astype(jnp.float32), pair_total, (((0,), (0,)), ((), ())), precision=HIGHEST
+    )
+    normed_grad = lax.all_gather(token_quarter, "tp", axis=1, tiled=True)
+    return gate_grad, up_grad, down_grad, normed_grad
 
 
 def shards(
@@ -198,64 +660,10 @@
     hidden = tokens.astype(jnp.float32)
     inverse = lax.rsqrt(jnp.mean(hidden * hidden, axis=1) + EPS)
     normed = (hidden * inverse[:, None] * norm_gain[None, :]).astype(jnp.bfloat16)
-    route_flat = routes.reshape(-1)
-    member = (route_flat[:, None] == jnp.arange(experts_count, dtype=jnp.int32)[None, :]).astype(
-        jnp.int32
-    )
-    earlier_count = jnp.sum((jnp.cumsum(member, axis=0) - member) * member, axis=1)
-    places = (route_flat * capacity + earlier_count).reshape(tok_rows, 2)
-    slot_ids = jnp.arange(experts_count * capacity, dtype=jnp.int32)[:, None]
-    first_hit = slot_ids == places[None, :, 0]
-    second_hit = slot_ids == places[None, :, 1]
-    placing = jnp.logical_or(first_hit, second_hit)
-    place_matrix = placing.astype(jnp.bfloat16)
-    slot_weight = jnp.sum(
-        jnp.where(first_hit, route_weight[None, :, 0], 0.0)
-        + jnp.where(second_hit, route_weight[None, :, 1], 0.0),
-        axis=1,
-    )
-    send_in = jnp.dot(place_matrix, normed, preferred_element_type=jnp.float32).astype(jnp.bfloat16)
-    send_cot = (
-        slot_weight[:, None] * jnp.dot(place_matrix, cotangent, preferred_element_type=jnp.float32)
-    ).astype(jnp.bfloat16)
-    half_cap = capacity // 2
-    part_in, part_cot = (
-        lax.all_to_all(
-            send_in.reshape(sp_count, half_cap, D), "sp", split_axis=0, concat_axis=0, tiled=True
-        ),
-        lax.all_to_all(
-            send_cot.reshape(sp_count, half_cap, D), "sp", split_axis=0, concat_axis=0, tiled=True
-        ),
-    )
-    other_in, other_cot = swapped((part_in, part_cot), "sp", 0)
-    lower_bit = lax.axis_index("sp") % 2 == 0
-    recv_in = jnp.concatenate(
-        [jnp.where(lower_bit, part_in, other_in), jnp.where(lower_bit, other_in, part_in)], axis=1
-    )
-    recv_cot = jnp.concatenate(
-        [jnp.where(lower_bit, part_cot, other_cot), jnp.where(lower_bit, other_cot, part_cot)],
-        axis=1,
-    )
-    rows_in = recv_in.reshape(-1, D)
-    rows_cot = recv_cot.reshape(-1, D)
-    gate_grad, up_grad, down_grad, input_part = expert_grads(
-        rows_in, rows_cot, gate_weight[0], up_weight[0], down_weight[0]
-    )
-    input_quarter = lax.psum_scatter(input_part, "tp", scatter_dimension=1, tiled=True)
-    returned = lax.all_to_all(
-        input_quarter.reshape(sp_count, capacity, quarter),
-        "sp",
-        split_axis=0,
-        concat_axis=0,
-        tiled=True,
-    )
-    pair_total = jnp.sum(returned.reshape(experts_count, 2, capacity, quarter), axis=1).reshape(
-        -1, quarter
-    )
-    token_quarter = lax.dot_general(
-        placing.astype(jnp.float32), pair_total, (((0,), (0,)), ((), ())), precision=HIGHEST
-    )
-    normed_grad = lax.all_gather(token_quarter, "tp", axis=1, tiled=True)
+    work = dense_grads if capacity == tok_rows and tp_count == 4 else routed_grads
+    gate_grad, up_grad, down_grad, normed_grad = work(
+        normed, cotangent, routes, route_weight, gate_weight[0], up_weight[0], down_weight[0]
+    )
     gained = norm_gain[None, :] * normed_grad
     dotted = jnp.sum(hidden * gained, axis=1)
     residual = (

time: 454 us -> 244 us (0.54)
  waiting for transfers between devices: 296 us -> 0.02 us
  Pallas kernels: 0 us -> 98.6 us
  starting transfers between devices: 21 us -> 0.04 us
  other arithmetic: 13.3 us -> 19.4 us
    all_to_all x3 -> x0, waiting for transfers between devices: 140 us -> none  [the longest x1 47.8 us: shards(): lax.all_to_all(input_quarter.reshape(sp_count, capacity, quarter), 'sp',...]
    pallas_call x0 -> x2, Pallas kernels: none -> 98.6 us  [the longest x1 59.5 us: gather_rows(): pl.pallas_call(functools.partial(gather_kernel, nz), out_shape=(whole, wh...]
    reduce_scatter x1 -> x0, waiting for transfers between devices: 71.4 us -> none  [shards(): lax.psum_scatter(input_part, 'tp', scatter_dimension=1, tiled=True)]
    ppermute x2 -> x0, waiting for transfers between devices: 65 us -> none  [swapped(): return lax.ppermute(value, axis, pairs)]
    reduce_scatter x1, waiting for transfers between devices: 20.1 us -> 0.01 us  [shards(): lax.psum_scatter(lax.dot_general(residual_grad, gated, (((0,), (0,)), (()...]
    all_to_all x3 -> x0, starting transfers between devices: 17.4 us -> none  [the longest x1 7.41 us: shards(): lax.all_to_all(send_in.reshape(sp_count, half_cap, D), 'sp', split_axis=0...]
    dot_general x3 -> x0, matrix products: 6.46 us -> none  [the longest x1 3.13 us: shards(): jnp.dot(place_matrix, normed, preferred_element_type=jnp.float32)]
    add x7, other arithmetic: 0.63 us -> 6.99 us  [compose(): nearer[1] + nearer[0][:, None, None] * higher[1]]
  transfers between devices with their start and end apart: 8 -> 1, of which waited for: 7 -> 0; matrix products, arithmetic and copies ran while one was open for 6% -> 11% of each run, Pallas kernels for 0% -> 0%
where the time goes in v1:
time: 244 us
  Pallas kernels  98.6 us (40%)
  blocking collectives  57.4 us (24%)
  matrix products  43.5 us (18%)
  other arithmetic  19.4 us (8%)
  between operations  15.2 us (6%)
  local copies, waits for them, and re-layouts  9.15 us (4%)
    pallas_call x1, Pallas kernels, gather_rows(): pl.pallas_call(functools.partial(gather_kernel, nz), out_shape=(whole, wh...  59.5 us
    pallas_call x1, Pallas kernels, total_rows(): pl.pallas_call(functools.partial(total_kernel, nz), out_shape=jax.ShapeDt...  39.1 us
    all_gather x1, blocking collectives, prefix(): gathered = jax.tree.map(lambda a: lax.all_gather(a, axis), part)  35.6 us
    unnamed x1, blocking collectives  21.9 us
    add x7, other arithmetic, compose(): nearer[1] + nearer[0][:, None, None] * higher[1]  6.99 us
    dot_general x1, matrix products, expert_grads(): lax.dot_general(rows_cot, down_mat, contract_cols, preferred_element_type...  6.47 us
    dot_general x1, matrix products, expert_grads(): lax.dot_general(rows_in, up_pre_grad, contract_rows, preferred_element_ty...  5.68 us
    dot_general x1, matrix products, expert_grads(): gate_pre = jnp.dot(rows_in, gate_mat, preferred_element_type=jnp.float32)  5.66 us
  transfers between devices with their start and end apart: 1, of which 0 were waited for; matrix products, arithmetic and copies ran while one was open for 11% of the time, Pallas kernels for 0%

profile of v1, /device:TPU:0, one launch (start us, length us, event | category | flops | bytes accessed | tf_op | source)
XLA Modules:
  0.0 243.6 jit_solution(2709629139913830129)
XLA Ops:
  7.9 1.2 fusion.24
  9.8 0.8 slice_bitcast_fusion.3
  13.7 1.3 convert_element_type.91
  15.0 1.3 convert_element_type.92
  16.4 0.9 copy.39
  17.3 1.6 copy.40
  18.9 2.0 fusion.26.a_ref
  21.5 59.5 %gather_rows.1 = (bf16[1024,2048]{1,0:T(8,128)(2,1)}, bf16[1024,2048]{1,0:T(8,128)(2,1)}, f32[8,4,128]{2,1,0:T(4,128)}) custom-call(bf16[128,2048]{1,0:T(8,128)(2,1)} %fusion.26.a_ref, bf16[128,2048]{1,0:T(8,128)(2,1)} %b_ref.1, f32[4,128]{1,0:T(4,128)} %select_add_fusion.w_ref), custom_call_target="tpu_custom_call" | custom-call | tf_op jit(solution)/shard_map/gather_rows/pallas_call | solution.py:383
  81.0 5.7 %fusion.5 = f32[1024,448]{0,1:T(8,128)} fusion(bf16[1024,2048]{1,0:T(8,128)(2,1)} %get-tuple-element.98, bf16[1,2048,448]{1,2,0:T(8,128)(2,1)S(1)} %copy-done), kind=kOutput, calls=%fused_computation.12 | convolution fusion | flops 1879048192 | bytes 7864320 | tf_op jit(solution)/shard_map/dot_general | solution.py:147
  86.7 3.4 %fusion.8 = f32[1024,448]{0,1:T(8,128)} fusion(bf16[1024,2048]{1,0:T(8,128)(2,1)S(1)} %copy-done.23, bf16[1,2048,448]{1,2,0:T(8,128)(2,1)S(1)} %copy-done.25), kind=kOutput, calls=%fused_computation.15 | convolution fusion | flops 1879048192 | bytes 7864320 | tf_op jit(solution)/shard_map/dot_general | solution.py:148
  90.8 6.5 %multiply_convert_fusion.2 = (bf16[1024,448]{0,1:T(8,128)(2,1)S(1)}, bf16[1024,448]{0,1:T(8,128)(2,1)S(1)}) fusion(f32[1024,448]{0,1:T(8,128)} %fusion.5, f32[1024,448]{0,1:T(8,128)} %fusion.8, bf16[1,448,2048]{2,1,0:T(8,128)(2,1)} %param.25, bf16[1024,2048]{1,0:T(8,128)(2,1)} %get-tuple-element.97, f32[1024]{0:T(1024)S(1)} %bitcast.130), kind=kOutput, calls=%fused_computation.20 | convolution fusion | flops 1891303424 | bytes 11538432 | tf_op jit(solution)/shard_map/dot_general | solution.py:152
  97.3 2.4 fusion.3
  99.7 4.6 %add_convert_fusion.p_ref = bf16[1024,2048]{1,0:T(8,128)(2,1)} fusion(f32[1024,2048]{1,0:T(8,128)S(1)} %fusion.3, bf16[1024,448]{0,1:T(8,128)(2,1)S(1)} %get-tuple-element.139, bf16[1,2048,448]{1,2,0:T(8,128)(2,1)S(1)} %copy-done.26), kind=kOutput, calls=%fused_computation.2 | convolution fusion | flops 1883242496 | bytes 15335424 | tf_op jit(solution)/shard_map/dot_general | solution.py:168
  104.4 39.1 %total_rows.1 = bf16[128,2048]{1,0:T(8,128)(2,1)} custom-call(bf16[1024,2048]{1,0:T(8,128)(2,1)} %add_convert_fusion.p_ref), custom_call_target="tpu_custom_call" | custom-call | tf_op jit(solution)/shard_map/total_rows/pallas_call | solution.py:524
  143.6 1.4 fusion.27
  145.0 1.5 fusion.29
  148.7 1.9 fusion.52
  152.2 21.9 %all-reduce = f32[32]{0:T(128)S(1)} all-reduce(f32[32]{0:T(128)S(1)} %dynamic-update-slice), channel_id=3, replica_groups=mesh['sp'=8,'tp'=4] {'sp'}, use_global_device_ids=true, to_apply=%add | all-reduce | flops 32 | bytes 256
  175.2 35.6 %all-gather = f32[32,64,64]{2,1,0:T(8,128)} all-gather(f32[4,64,64]{2,1,0:T(8,128)S(1)} %fusion.33), channel_id=2, replica_groups=mesh['sp'=8,'tp'=4] {'sp'}, dimensions={0}, use_global_device_ids=true | all-gather | bytes 589824 | tf_op jit(solution)/shard_map/all_gather | solution.py:30
  210.8 7.3 %while.14 = (s32[]{:T(128)}, f32[4,64,64]{2,1,0:T(8,128)S(1)}, s32[]{:T(128)}, f32[8,4,64,64]{3,2,1,0:T(8,128)}, f32[8,4]{1,0:T(8,128)S(1)}, /*index=5*/s32[]{:T(128)}, s32[]{:T(128)}, s32[]{:T(128)}, s32[]{:T(128)}) while((s32[]{:T(128)}, f32[4,64,64]{2,1,0:T(8,128)S(1)}, s32[]{:T(128)}, f32[8,4,64,64]{3,2,1,0:T(8,128)}, ...), condition=%wide.region_5.6_spmd, body=%wide.region_4.5_spmd.sunk | while | flops 32774 | bytes 196811 | solution.py:39
  210.9 1.0 bitcast_add_fusion.2
  211.9 1.0 bitcast_add_fusion.2
  212.9 1.0 bitcast_add_fusion.2
  214.0 1.0 bitcast_add_fusion.2
  215.0 1.0 bitcast_add_fusion.2
  216.0 1.0 bitcast_add_fusion.2
  217.1 1.0 bitcast_add_fusion.2
  221.2 1.2 fusion.23
  222.8 0.9 fusion.22
  223.7 5.7 %fusion.2 = bf16[1,2048,448]{1,2,0:T(8,128)(2,1)} fusion(bf16[1024,448]{0,1:T(8,128)(2,1)S(1)} %copy-done.31, bf16[1024,2048]{1,0:T(8,128)(2,1)} %get-tuple-element.98), kind=kOutput, calls=%fused_computation.9 | convolution fusion | flops 1879965696 | bytes 6946816 | tf_op jit(solution)/shard_map/dot_general | solution.py:162
  229.5 3.3 %fusion.1 = bf16[1,2048,448]{1,2,0:T(8,128)(2,1)} fusion(bf16[1024,448]{0,1:T(8,128)(2,1)S(1)} %copy-done.29, bf16[1024,2048]{1,0:T(8,128)(2,1)S(1)} %copy-done.24), kind=kOutput, calls=%fused_computation.8 | convolution fusion | flops 1879965696 | bytes 6946816 | tf_op jit(solution)/shard_map/dot_general | solution.py:159
  233.2 3.6 %fusion = bf16[1,448,2048]{2,1,0:T(8,128)(2,1)} fusion(bf16[1024,2048]{1,0:T(8,128)(2,1)S(1)} %copy-done.22, f32[1024]{0:T(1024)S(1)} %bitcast.131, f32[1024,448]{0,1:T(8,128)S(1)} %copy-done.33, f32[1024,448]{0,1:T(8,128)S(1)} %copy-done.32), kind=kOutput, calls=%fused_computation.7 | convolution fusion | flops 1889009664 | bytes 9703424 | tf_op jit(solution)/shard_map/dot_general | solution.py:151
  (107 shorter events, 13.9 us)
Async XLA Ops:
  7.2 73.8 %copy-start = (bf16[1,2048,448]{1,2,0:T(8,128)(2,1)S(1)}, bf16[1,2048,448]{1,2,0:T(8,128)(2,1)}, u32[]{:S(2)}) copy-start(bf16[1,2048,448]{1,2,0:T(8,128)(2,1)} %param.23) | copy-start | bytes 5505028
  7.2 229.6 %reduce-scatter.2.cloned.1.call-start = ((), (), s32[]{:S(2)}) async-start(), calls=%async_computation.1 | async-start | bytes 2359296 | tf_op jit(solution)/shard_map/reduce_scatter | solution.py:702
  9.1 77.6 %copy-start.20 = (f32[128]{0:T(128)}, f32[128]{0:T(128)S(1)}, u32[]{:S(2)}) copy-start(f32[128]{0:T(128)S(1)} %add_rsqrt_fusion) | copy-start | bytes 1540
  81.0 5.7 %copy-start.23 = (bf16[1024,2048]{1,0:T(8,128)(2,1)S(1)}, bf16[1024,2048]{1,0:T(8,128)(2,1)}, u32[]{:S(2)}) copy-start(bf16[1024,2048]{1,0:T(8,128)(2,1)} %get-tuple-element.98) | copy-start | bytes 12582916
  81.0 5.7 %copy-start.25 = (bf16[1,2048,448]{1,2,0:T(8,128)(2,1)S(1)}, bf16[1,2048,448]{1,2,0:T(8,128)(2,1)}, u32[]{:S(2)}) copy-start(bf16[1,2048,448]{1,2,0:T(8,128)(2,1)} %param.24) | copy-start | bytes 5505028
  90.8 6.5 %copy-start.18 = (f32[8,1,128]{2,1,0:T(1,128)}, f32[8,1,128]{2,1,0:T(1,128)S(1)}, u32[]{:S(2)}) copy-start(f32[8,1,128]{2,1,0:T(1,128)S(1)} %constant_dynamic-slice_fusion.1) | copy-start | bytes 12292
  97.3 2.4 %copy-start.28 = (bf16[1024,448]{0,1:T(8,128)(2,1)}, bf16[1024,448]{0,1:T(8,128)(2,1)S(1)}, u32[]{:S(2)}) copy-start(bf16[1024,448]{0,1:T(8,128)(2,1)S(1)} %get-tuple-element.140) | copy-start | bytes 2752516
  104.4 39.1 %copy-start.1 = (bf16[128,2048]{1,0:T(8,128)(2,1)S(1)}, bf16[128,2048]{1,0:T(8,128)(2,1)}, u32[]{:S(2)}) copy-start(bf16[128,2048]{1,0:T(8,128)(2,1)} %param.18) | copy-start | bytes 1572868
  104.4 39.1 %copy-start.11 = (f32[2048]{0:T(1024)S(1)}, f32[2048]{0:T(1024)}, u32[]{:S(2)}) copy-start(f32[2048]{0:T(1024)} %param.19) | copy-start | bytes 24580
  104.4 40.6 %copy-start.2 = (bf16[128,2048]{1,0:T(8,128)(2,1)S(1)}, bf16[128,2048]{1,0:T(8,128)(2,1)}, u32[]{:S(2)}) copy-start(bf16[128,2048]{1,0:T(8,128)(2,1)} %b_ref.1) | copy-start | bytes 1572868
  143.5 3.0 %copy-start.4 = (f32[1,4,64,64]{3,2,1,0:T(8,128)S(1)}, f32[1,4,64,64]{3,2,1,0:T(8,128)}, u32[]{:S(2)}) copy-start(f32[1,4,64,64]{3,2,1,0:T(8,128)} %param.32) | copy-start | bytes 196612
  143.5 3.0 %copy-start.6 = (f32[128,64]{0,1:T(8,128)S(1)}, f32[128,64]{0,1:T(8,128)}, u32[]{:S(2)}) copy-start(f32[128,64]{0,1:T(8,128)} %convert_element_type.91) | copy-start | bytes 98308
  143.5 3.0 %copy-start.15 = (f32[128,4]{0,1:T(4,128)S(1)}, f32[128,4]{0,1:T(4,128)}, u32[]{:S(2)}) copy-start(f32[128,4]{0,1:T(4,128)} %get-tuple-element.145) | copy-start | bytes 6148
  143.5 3.3 %copy-start.9 = (f32[128,64]{0,1:T(8,128)S(1)}, f32[128,64]{0,1:T(8,128)}, u32[]{:S(2)}) copy-start(f32[128,64]{0,1:T(8,128)} %convert_element_type.92) | copy-start | bytes 98308
  143.5 3.3 %copy-start.12 = (pred[128,128]{1,0:T(8,128)(4,1)S(1)}, pred[128,128]{1,0:T(8,128)(4,1)}, u32[]{:S(2)}) copy-start(pred[128,128]{1,0:T(8,128)(4,1)} %iota_compare_fusion) | copy-start | bytes 49156
  143.6 3.9 %copy-start.3 = (bf16[2048,256]{1,0:T(8,128)(2,1)S(1)}, bf16[2048,256]{1,0:T(8,128)(2,1)}, u32[]{:S(2)}) copy-start(bf16[2048,256]{1,0:T(8,128)(2,1)} %param.33) | copy-start | bytes 3145732
  145.0 3.0 %copy-start.8 = (f32[128,256]{0,1:T(8,128)S(1)}, f32[128,256]{0,1:T(8,128)}, u32[]{:S(2)}) copy-start(f32[128,256]{0,1:T(8,128)} %copy.40) | copy-start | bytes 393220
  145.0 3.0 %copy-start.14 = (f32[4,128]{1,0:T(4,128)S(1)}, f32[4,128]{1,0:T(4,128)}, u32[]{:S(2)}) copy-start(f32[4,128]{1,0:T(4,128)} %param.28) | copy-start | bytes 6148
  148.7 3.2 %copy-start.21 = (f32[4]{0:T(128)S(1)}, f32[4]{0:T(128)}, u32[]{:S(2)}) copy-start(f32[4]{0:T(128)} %get-tuple-element.128) | copy-start | bytes 52
  148.7 26.1 %copy-start.7 = (f32[128,64]{0,1:T(8,128)S(1)}, f32[128,64]{0,1:T(8,128)}, u32[]{:S(2)}) copy-start(f32[128,64]{0,1:T(8,128)} %convert_element_type.91) | copy-start | bytes 98308
  148.7 26.1 %copy-start.16 = (f32[128,4]{0,1:T(4,128)S(1)}, f32[128,4]{0,1:T(4,128)}, u32[]{:S(2)}) copy-start(f32[128,4]{0,1:T(4,128)} %get-tuple-element.145) | copy-start | bytes 6148
  175.2 42.9 %copy-start.10 = (f32[128,64]{0,1:T(8,128)S(1)}, f32[128,64]{0,1:T(8,128)}, u32[]{:S(2)}) copy-start(f32[128,64]{0,1:T(8,128)} %convert_element_type.92) | copy-start | bytes 98308
  175.2 42.9 %copy-start.17 = (f32[128,4]{0,1:T(4,128)S(1)}, f32[128,4]{0,1:T(4,128)}, u32[]{:S(2)}) copy-start(f32[128,4]{0,1:T(4,128)} %get-tuple-element.144) | copy-start | bytes 6148
  210.8 9.4 %copy-start.5 = (f32[1,4,64,64]{3,2,1,0:T(8,128)S(1)}, f32[1,4,64,64]{3,2,1,0:T(8,128)}, u32[]{:S(2)}) copy-start(f32[1,4,64,64]{3,2,1,0:T(8,128)} %param.32) | copy-start | bytes 196612
  210.8 9.8 %copy-start.13 = (pred[128,128]{1,0:T(8,128)(4,1)S(1)}, pred[128,128]{1,0:T(8,128)(4,1)}, u32[]{:S(2)}) copy-start(pred[128,128]{1,0:T(8,128)(4,1)} %iota_compare_fusion) | copy-start | bytes 49156
  219.5 4.3 %copy-start.31 = (bf16[1024,448]{0,1:T(8,128)(2,1)S(1)}, bf16[1024,448]{0,1:T(8,128)(2,1)}, u32[]{:S(2)}) copy-start(bf16[1024,448]{0,1:T(8,128)(2,1)} %copy-done.30) | copy-start | bytes 2752516
  223.7 5.7 %copy-start.24 = (bf16[1024,2048]{1,0:T(8,128)(2,1)S(1)}, bf16[1024,2048]{1,0:T(8,128)(2,1)}, u32[]{:S(2)}) copy-start(bf16[1024,2048]{1,0:T(8,128)(2,1)} %get-tuple-element.98) | copy-start | bytes 12582916
  223.7 5.7 %copy-start.29 = (bf16[1024,448]{0,1:T(8,128)(2,1)S(1)}, bf16[1024,448]{0,1:T(8,128)(2,1)}, u32[]{:S(2)}) copy-start(bf16[1024,448]{0,1:T(8,128)(2,1)} %copy-done.28) | copy-start | bytes 2752516
  229.4 3.4 %copy-start.19 = (f32[8,1,128]{2,1,0:T(1,128)S(1)}, f32[8,1,128]{2,1,0:T(1,128)}, u32[]{:S(2)}) copy-start(f32[8,1,128]{2,1,0:T(1,128)} %copy-done.18) | copy-start | bytes 12292
  229.4 3.4 %copy-start.22 = (bf16[1024,2048]{1,0:T(8,128)(2,1)S(1)}, bf16[1024,2048]{1,0:T(8,128)(2,1)}, u32[]{:S(2)}) copy-start(bf16[1024,2048]{1,0:T(8,128)(2,1)} %get-tuple-element.97) | copy-start | bytes 12582916
  229.4 3.3 %copy-start.32 = (f32[1024,448]{0,1:T(8,128)S(1)}, f32[1024,448]{0,1:T(8,128)}, u32[]{:S(2)}) copy-start(f32[1024,448]{0,1:T(8,128)} %fusion.5) | copy-start | bytes 5505028
  229.5 3.7 %copy-start.33 = (f32[1024,448]{0,1:T(8,128)S(1)}, f32[1024,448]{0,1:T(8,128)}, u32[]{:S(2)}) copy-start(f32[1024,448]{0,1:T(8,128)} %fusion.8) | copy-start | bytes 5505028
  (3 other events, 6.8 us)
Sparse Core Ops, SparseCore 0:
  150.8 75.7 reduce-scatter.1

commit v2 on v1

--- a/solution.py
+++ b/solution.py
@@ -197,7 +197,21 @@
 
 
 def gather_kernel(
-    nz, a_ref, b_ref, w_ref, oa_ref, ob_ref, ow_ref, own_sem, z_send, z_recv, x_sem, y_sem, c_sem, d_sem, w_sem
+    nz,
+    a_ref,
+    b_ref,
+    w_ref,
+    oa_ref,
+    ob_ref,
+    ow_ref,
+    own_sem,
+    z_send,
+    z_recv,
+    x_sem,
+    y_sem,
+    c_sem,
+    d_sem,
+    w_sem,
 ):
     rows = a_ref.shape[0]
     part = rows // 4
@@ -210,66 +224,23 @@
     peers = [((sp + k) % count, tp) for k in range(1, count)]
     greet(peers + [over_y, over_c])
 
-    def span(core, row, whole):
-        if whole:
-            return core * (2 * part), 2 * part
-        return core * (2 * part) + row * part, part
-
-    def copies(block, piece, send, recv, device, own=False):
-        start, size = piece
-        made = []
-        for k, (src, dst) in enumerate(((a_ref, oa_ref), (b_ref, ob_ref))):
-            at = pl.ds(pl.multiple_of(block * rows + start, part), size)
-            source = src.at[pl.ds(pl.multiple_of(start, part), size)] if own else dst.at[at]
-            made.append(remote(source, dst.at[at], send.at[k, block], recv.at[k, block], device))
-        return made
-
-    def go(made):
-        for copy in made:
-            copy.start()
-
-    def arrived(made):
-        for copy in made:
-            copy.wait_recv()
-
-    def sent(made):
-        for copy in made:
-            copy.wait_send()
-
-    mine_half = span(c, y, True)
-    mine_part = span(c, y, False)
-    y_part = span(c, 1 - y, False)
-    for k in range(1, count):
-        other = ((sp + k) % count, tp)
-        remote(w_ref, ow_ref.at[sp], w_sem.at[0, k], w_sem.at[1, k], other).start()
-    steps = []
-
-    def send_if(condition, make):
-        if condition is None:
-            go(make())
-        else:
-            @pl.when(condition)
-            def _():
-                go(make())
-        steps.append((condition, make))
-
+    mine = (c * 2 + y) * part
+    beside = (c * 2 + 1 - y) * part
+    mine_other = ((1 - c) * 2 + y) * part
+    beside_other = ((1 - c) * 2 + 1 - y) * part
+    pairs = ((a_ref, oa_ref), (b_ref, ob_ref))
+    own = z * 2 + x
     up = (jnp.minimum(z + 1, nz - 1) * 2 + x, tp)
     down = (jnp.maximum(z - 1, 0) * 2 + x, tp)
-    own = z * 2 + x
-    send_if(z < nz - 1, lambda: copies(own, mine_half, z_send.at[0], z_recv, up, True))
-    send_if(z > 0, lambda: copies(own, mine_half, z_send.at[1], z_recv, down, True))
-    send_if(None, lambda: copies(own, mine_half, x_sem.at[0], x_sem.at[1], over_x, True))
-    locals_ = [
-        pltpu.make_async_copy(src, dst.at[pl.ds(pl.multiple_of(own * rows, rows), rows)], own_sem.at[k])
-        for k, (src, dst) in enumerate(((a_ref, oa_ref), (b_ref, ob_ref)))
-    ]
-    locals_.append(pltpu.make_async_copy(w_ref, ow_ref.at[sp], own_sem.at[2]))
-    go(locals_)
-
-    def sides(step):
-        if step == 0:
-            return [(None, z, 0)]
-        return [(z - step >= 0, z - step, 0), (z + step <= nz - 1, z + step, 1)]
+    sends = []
+
+    def piece(k, block, start, sems, device):
+        src, dst = pairs[k]
+        at = dst.at[pl.ds(pl.multiple_of(block * rows + start, part), part)]
+        source = at
+        if block is own:
+            source = src.at[pl.ds(pl.multiple_of(start, part), part)]
+        return remote(source, at, sems[0].at[k, block], sems[1].at[k, block], device)
 
     def guarded(condition, work):
         if condition is None:
@@ -277,100 +248,106 @@
         else:
             pl.when(condition)(work)
 
-    def from_z(step):
+    def send(condition, *what):
+        guarded(condition, lambda: piece(*what).start())
+        sends.append((condition, what))
+
+    def take(condition, *what):
+        guarded(condition, lambda: piece(*what).wait_recv())
+
+    z_up, z_down = (z_send.at[0], z_recv.at[0]), (z_send.at[1], z_recv.at[0])
+    z_up_late, z_down_late = (z_send.at[2], z_recv.at[1]), (z_send.at[3], z_recv.at[1])
+    over_x_sems, over_x_late = (x_sem.at[0], x_sem.at[1]), (x_sem.at[2], x_sem.at[3])
+    over_y_sems = (y_sem.at[0], y_sem.at[1])
+    core_mine, core_beside = (c_sem.at[0], c_sem.at[1]), (d_sem.at[0], d_sem.at[1])
+    for k in range(2):
+        send(z < nz - 1, k, own, mine, z_up, up)
+        send(z > 0, k, own, mine, z_down, down)
+        send(None, k, own, mine, over_x_sems, over_x)
+    for k in range(1, count):
+        other = ((sp + k) % count, tp)
+        remote(w_ref, ow_ref.at[sp], w_sem.at[0, k], w_sem.at[1, k], other).start()
+    locals_ = [
+        pltpu.make_async_copy(src, dst.at[pl.ds(pl.multiple_of(own * rows, rows), rows)], own_sem.at[k])
+        for k, (src, dst) in enumerate(pairs)
+    ]
+    locals_.append(pltpu.make_async_copy(w_ref, ow_ref.at[sp], own_sem.at[2]))
+    for copy in locals_:
+        copy.start()
+
+    def sides(step):
+        if step == 0:
+            return [(None, z, 0)]
+        return [(z - step >= 0, z - step, 0), (z + step <= nz - 1, z + step, 1)]
+
+    def from_z(k, step):
         for condition, at, way in sides(step):
             block = at * 2 + x
-            piece = mine_half if step == 1 else mine_part
-            guarded(condition, lambda: arrived(copies(block, piece, z_send.at[way], z_recv, up)))
-            onward = jnp.logical_and(condition, z < nz - 1 if way == 0 else z > 0)
-            target = up if way == 0 else down
-            send_if(
-                onward,
-                lambda block=block, way=way, target=target: copies(
-                    block, mine_part, z_send.at[way], z_recv, target
-                ),
-            )
-            send_if(
-                condition,
-                lambda block=block: copies(block, mine_part, x_sem.at[0], x_sem.at[1], over_x),
-            )
+            take(condition, k, block, mine, z_up, up)
+            if step < nz - 1:
+                onward = jnp.logical_and(condition, z < nz - 1 if way == 0 else z > 0)
+                send(onward, k, block, mine, (z_up, z_down)[way], (up, down)[way])
+            send(condition, k, block, mine, over_x_sems, over_x)
             if step >= 2:
-                send_if(
-                    condition,
-                    lambda block=block: copies(block, mine_part, y_sem.at[0], y_sem.at[1], over_y),
-                )
-            send_if(
-                condition,
-                lambda block=block, piece=piece: copies(
-                    block, piece, c_sem.at[0], c_sem.at[1], over_c
-                ),
-            )
-
-    def from_x(step):
+                send(condition, k, block, mine, over_y_sems, over_y)
+            send(condition, k, block, mine, core_mine, over_c)
+
+    def from_x(k, step):
         for condition, at, way in sides(step):
             block = at * 2 + 1 - x
-            piece = mine_half if step == 0 else mine_part
-            guarded(
-                condition,
-                lambda: arrived(copies(block, piece, x_sem.at[0], x_sem.at[1], over_x)),
-            )
+            take(condition, k, block, mine, over_x_sems, over_x)
             if step >= 1:
-                send_if(
-                    condition,
-                    lambda block=block: copies(block, mine_part, y_sem.at[0], y_sem.at[1], over_y),
-                )
-            send_if(
-                condition,
-                lambda block=block, piece=piece: copies(
-                    block, piece, c_sem.at[0], c_sem.at[1], over_c
-                ),
-            )
-
-    def from_y(step, column):
+                send(condition, k, block, mine, over_y_sems, over_y)
+            send(condition, k, block, mine, core_mine, over_c)
+
+    def from_y(k, step, column):
         for condition, at, way in sides(step):
             block = at * 2 + column
-            guarded(
-                condition,
-                lambda: arrived(copies(block, y_part, y_sem.at[0], y_sem.at[1], over_y)),
-            )
-            send_if(
-                condition,
-                lambda block=block: copies(block, y_part, d_sem.at[0], d_sem.at[1], over_c),
-            )
-
+            take(condition, k, block, beside, over_y_sems, over_y)
+            send(condition, k, block, beside, core_beside, over_c)
+
+    def late(k):
+        send(z < nz - 1, k, own, beside, z_up_late, up)
+        send(z > 0, k, own, beside, z_down_late, down)
+        send(None, k, own, beside, over_x_late, over_x)
+
+    def from_late(k):
+        take(None, k, z * 2 + 1 - x, beside, over_x_late, over_x)
+        send(None, k, z * 2 + 1 - x, beside, core_beside, over_c)
+        for condition, at, way in sides(1):
+            take(condition, k, at * 2 + x, beside, z_up_late, up)
+            send(condition, k, at * 2 + x, beside, core_beside, over_c)
+
+    defer = max(nz - 2, 0)
     for step in range(nz + 2):
-        if 1 <= step < nz:
-            from_z(step)
-        if 0 <= step - 1 < nz:
-            from_x(step - 1)
-        if 2 <= step - 1 < nz:
-            from_y(step - 1, x)
-        if 1 <= step - 2 < nz:
-            from_y(step - 2, 1 - x)
-
-    for step in range(nz):
-        for condition, at, way in sides(step):
-            for column, first, then in ((x, 1, 2), (1 - x, 0, 1)):
-                block = at * 2 + column
-                if step >= first:
-                    piece = span(1 - c, y, step == first)
-                    guarded(
-                        condition,
-                        lambda: arrived(copies(block, piece, c_sem.at[0], c_sem.at[1], over_c)),
-                    )
-                if step >= then:
-                    piece = span(1 - c, 1 - y, False)
-                    guarded(
-                        condition,
-                        lambda: arrived(copies(block, piece, d_sem.at[0], d_sem.at[1], over_c)),
-                    )
+        for k in range(2):
+            if 1 <= step < nz:
+                from_z(k, step)
+            if step == defer:
+                late(k)
+            if 0 <= step - 1 < nz:
+                from_x(k, step - 1)
+            if 2 <= step - 1 < nz:
+                from_y(k, step - 1, x)
+            if 1 <= step - 2 < nz:
+                from_y(k, step - 2, 1 - x)
+    for k in range(2):
+        from_late(k)
+    for k in range(2):
+        for step in range(nz):
+            for condition, at, way in sides(step):
+                for column in (x, 1 - x):
+                    if step >= 1 or column is not x:
+                        block = at * 2 + column
+                        take(condition, k, block, mine_other, core_mine, over_c)
+                        take(condition, k, block, beside_other, core_beside, over_c)
     for k in range(1, count):
         source = (sp + count - k) % count
         remote(w_ref, ow_ref.at[source], w_sem.at[0, k], w_sem.at[1, k], over_x).wait_recv()
     for k in range(1, count):
         remote(w_ref, ow_ref.at[sp], w_sem.at[0, k], w_sem.at[1, k], over_x).wait_send()
-    for condition, make in steps:
-        guarded(condition, lambda: sent(make()))
+    for condition, what in sends:
+        guarded(condition, lambda: piece(*what).wait_send())
     for copy in locals_:
         copy.wait()
 
@@ -387,9 +364,9 @@
         out_specs=(pl.BlockSpec(memory_space=pl.ANY),) * 3,
         scratch_shapes=[
             dma((3,)),
+            dma((4, 2, count)),
             dma((2, 2, count)),
-            dma((2, count)),
-            dma((2, 2, count)),
+            dma((4, 2, count)),
             dma((2, 2, count)),
             dma((2, 2, count)),
             dma((2, 2, count)),
@@ -548,21 +525,129 @@
     )(parts)
 
 
-def dense_grads(normed, cotangent, routes, route_weight, gate_mat, up_mat, down_mat):
+def carry_kernel(
+    nz, coef_ref, carry_ref, p_ref, later_ref, o_ref, rc, px, sx, pz, r_sem, x_sem, z_sem
+):
+    count = 2 * nz
+    rows = p_ref.shape[0] // count
+    heads = coef_ref.shape[1]
+    per_head = carry_ref.shape[0] // heads
+    sp, tp = lax.axis_index("sp"), lax.axis_index("tp")
+    z, x = sp // 2, sp % 2
+    over_x = (z * 2 + 1 - x, tp)
+    f32, bf16 = jnp.float32, jnp.bfloat16
+    greet([((sp + k) % count, tp) for k in range(1, count)])
+
+    def block(index):
+        return pl.ds(pl.multiple_of(index * rows, rows), rows)
+
+    def plane(i):
+        return (z + 1 + i) % nz
+
+    firsts, along = [], []
+    for i in range(nz):
+        copy = remote(
+            p_ref.at[block(plane(i) * 2 + 1 - x)],
+            px.at[i],
+            x_sem.at[0, i],
+            x_sem.at[1, i],
+            over_x,
+        )
+        copy.start()
+        firsts.append(copy)
+
+    def carry_copy(d):
+        target = (jnp.maximum(sp - d, 0), tp)
+        return remote(carry_ref, rc.at[d], r_sem.at[0, d], r_sem.at[1, d], target)
+
+    for d in range(1, count):
+        pl.when(sp - d >= 0)(lambda: carry_copy(d).start())
+    total = None
+    for i in range(nz):
+        firsts[i].wait_recv()
+        value = p_ref[block(plane(i) * 2 + x)].astype(f32) + px[i].astype(f32)
+        if i < nz - 1:
+            sx[i] = value.astype(bf16)
+            copy = remote(
+                sx.at[i], pz.at[i], z_sem.at[0, i], z_sem.at[1, i], (plane(i) * 2 + x, tp)
+            )
+            copy.start()
+            along.append(copy)
+        else:
+            o_ref[...] = value
+    later_ref[...] = jnp.zeros_like(later_ref)
+    for d in range(1, count):
+
+        @pl.when(sp + d < count)
+        def _():
+            carry_copy(d).wait_recv()
+            for h in range(heads):
+                at = pl.ds(h * per_head, per_head)
+                later_ref[at] += coef_ref[d - 1, h] * rc[d, at].astype(f32)
+
+    for i in range(nz - 1):
+        along[i].wait_recv()
+        o_ref[...] += pz[i].astype(f32)
+    for copy in firsts + along:
+        copy.wait_send()
+    for d in range(1, count):
+        pl.when(sp - d >= 0)(lambda: carry_copy(d).wait_send())
+
+
+def carry_and_total(nz, decays, carried, parts):
+    count = 2 * nz
+    heads, channels, states = carried.shape
+    lanes = 128
+    place = lax.axis_index("sp")
+    padded = jnp.concatenate([decays, jnp.ones_like(decays)])
+    ahead = lax.dynamic_slice_in_dim(padded, place + 1, count - 1, 0)
+    coefs = jnp.concatenate([jnp.ones_like(ahead[:1]), jnp.cumprod(ahead[:-1], axis=0)])
+    flat = carried.astype(jnp.bfloat16).reshape(-1, lanes)
+    rows, width = parts.shape[0] // count, parts.shape[1]
+    dma = pltpu.SemaphoreType.DMA
+    vmem = functools.partial(pltpu.VMEM, dtype=jnp.bfloat16)
+    space = pl.BlockSpec(memory_space=pltpu.VMEM)
+    later, total = pl.pallas_call(
+        functools.partial(carry_kernel, nz),
+        out_shape=(
+            jax.ShapeDtypeStruct(flat.shape, jnp.float32),
+            jax.ShapeDtypeStruct((rows, width), jnp.float32),
+        ),
+        in_specs=[pl.BlockSpec(memory_space=pltpu.SMEM), space, space],
+        out_specs=(space, space),
+        scratch_shapes=[
+            vmem((count,) + flat.shape),
+            vmem((nz, rows, width)),
+            vmem((nz, rows, width)),
+            vmem((nz, rows, width)),
+            dma((2, count)),
+            dma((2, nz)),
+            dma((2, nz)),
+        ],
+        compiler_params=pltpu.CompilerParams(collective_id=2, has_side_effects=True),
+        name="carry_and_total",
+    )(coefs, flat, parts.astype(jnp.bfloat16))
+    return later.reshape(heads, channels, states), total
+
+
+def dense_grads(normed, cotangent, routes, route_weight, decay_now, gate_mat, up_mat, down_mat):
     sp_count = lax.axis_size("sp")
     experts_count = sp_count // 2
     nz = sp_count // 2
     names = jnp.arange(experts_count, dtype=jnp.int32)[:, None]
     table = jnp.where(routes[None, :, 0] == names, route_weight[None, :, 0], 0.0)
     table = table + jnp.where(routes[None, :, 1] == names, route_weight[None, :, 1], 0.0)
+    spread = jnp.broadcast_to(decay_now[:, None], (decay_now.shape[0], table.shape[1]))
+    table = jnp.concatenate([table, spread])
     rows_in, cot_all, tables = gather_rows(nz, normed, cotangent, table)
+    decays = tables[:, experts_count:, 0]
     weight_all = lax.dynamic_index_in_dim(tables, lax.axis_index("sp") // 2, 1, False).reshape(-1)
     rows_cot = (weight_all[:, None] * cot_all.astype(jnp.float32)).astype(jnp.bfloat16)
     gate_grad, up_grad, down_grad, input_part = expert_grads(
         rows_in, rows_cot, gate_mat, up_mat, down_mat
     )
     normed_grad = total_rows(nz, input_part.astype(jnp.bfloat16)).astype(jnp.float32)
-    return gate_grad, up_grad, down_grad, normed_grad
+    return gate_grad, up_grad, down_grad, normed_grad, decays
 
 
 def routed_grads(normed, cotangent, routes, route_weight, gate_mat, up_mat, down_mat):
@@ -660,10 +745,17 @@
     hidden = tokens.astype(jnp.float32)
     inverse = lax.rsqrt(jnp.mean(hidden * hidden, axis=1) + EPS)
     normed = (hidden * inverse[:, None] * norm_gain[None, :]).astype(jnp.bfloat16)
-    work = dense_grads if capacity == tok_rows and tp_count == 4 else routed_grads
-    gate_grad, up_grad, down_grad, normed_grad = work(
-        normed, cotangent, routes, route_weight, gate_weight[0], up_weight[0], down_weight[0]
-    )
+    dense = capacity == tok_rows and tp_count == 4
+    mats = (gate_weight[0], up_weight[0], down_weight[0])
+    if dense:
+        decay_now = jnp.exp(jnp.sum(-decay_rate[:, None] * step_size, axis=1))
+        gate_grad, up_grad, down_grad, normed_grad, decays = dense_grads(
+            normed, cotangent, routes, route_weight, decay_now, *mats
+        )
+    else:
+        gate_grad, up_grad, down_grad, normed_grad = routed_grads(
+            normed, cotangent, routes, route_weight, *mats
+        )
     gained = norm_gain[None, :] * normed_grad
     dotted = jnp.sum(hidden * gained, axis=1)
     residual = (
@@ -685,9 +777,16 @@
         mix_grad,
         per_group,
     )
-    totals, later_state = prefix(
-        (decay_now, carried), "sp", compose, (jnp.ones_like(decay_now), jnp.zeros_like(carried))
-    )
+    proj_part = lax.dot_general(
+        residual_grad, gated, (((0,), (0,)), ((), ())), preferred_element_type=jnp.float32
+    )
+    if dense:
+        later_state, out_proj_grad = carry_and_total(sp_count // 2, decays, carried, proj_part)
+    else:
+        totals, later_state = prefix(
+            (decay_now, carried), "sp", compose, (jnp.ones_like(decay_now), jnp.zeros_like(carried))
+        )
+        out_proj_grad = lax.psum_scatter(proj_part, "sp", scatter_dimension=0, tiled=True)
     scan_grad, write_grad, read_grad = block_back(
         scan_input,
         step_size,
@@ -698,14 +797,6 @@
         state_grad,
         later_state,
         per_group,
-    )
-    out_proj_grad = lax.psum_scatter(
-        lax.dot_general(
-            residual_grad, gated, (((0,), (0,)), ((), ())), preferred_element_type=jnp.float32
-        ),
-        "sp",
-        scatter_dimension=0,
-        tiled=True,
     )
     residual_part = lax.dynamic_slice_in_dim(
         residual_grad, lax.axis_index("tp") * quarter, quarter, 1

time: 244 us -> 175 us (0.72)
  blocking collectives: 57.4 us -> 0 us
  Pallas kernels: 98.6 us -> 115 us
  between operations: 15.2 us -> 1.07 us
  other arithmetic: 19.4 us -> 9.94 us
  matrix products: 43.5 us -> 36.5 us
    all_gather x1 -> x0, blocking collectives: 35.6 us -> none  [prefix(): gathered = jax.tree.map(lambda a: lax.all_gather(a, axis), part)]
    pallas_call x0 -> x1, Pallas kernels: none -> 24.8 us  [carry_and_total(): pl.pallas_call(functools.partial(carry_kernel, nz), out_shape=(jax.ShapeD...]
    unnamed x1 -> x0, blocking collectives: 21.9 us -> none
    pallas_call x1, Pallas kernels: 59.5 us -> 51.5 us  [gather_rows(): pl.pallas_call(functools.partial(gather_kernel, nz), out_shape=(whole, wh...]
    add x7 -> x0, other arithmetic: 6.99 us -> none  [compose(): nearer[1] + nearer[0][:, None, None] * higher[1]]
    dot_general x1, matrix products: 6.47 us -> 2.67 us  [expert_grads(): lax.dot_general(rows_cot, down_mat, contract_cols, preferred_element_type...]
  transfers between devices with their start and end apart: 1 -> 0, of which waited for: 0 -> 0; matrix products, arithmetic and copies ran while one was open for 11% -> 0% of each run, Pallas kernels for 0% -> 0%
where the time goes in v2:
time: 175 us; the launch traced here: 174 us
  Pallas kernels  115 us (66%)
  matrix products  36.5 us (21%)
  local copies, waits for them, and re-layouts  11.4 us (7%)
  other arithmetic  9.94 us (6%)
    pallas_call x1, Pallas kernels, gather_rows(): pl.pallas_call(functools.partial(gather_kernel, nz), out_shape=(whole, wh...  51.5 us
    pallas_call x1, Pallas kernels, total_rows(): pl.pallas_call(functools.partial(total_kernel, nz), out_shape=jax.ShapeDt...  39 us
    pallas_call x1, Pallas kernels, carry_and_total(): pl.pallas_call(functools.partial(carry_kernel, nz), out_shape=(jax.ShapeD...  24.8 us
    dot_general x1, matrix products, expert_grads(): gate_pre = jnp.dot(rows_in, gate_mat, preferred_element_type=jnp.float32)  4.43 us
    dot_general x1, matrix products, expert_grads(): lax.dot_general(up_pre_grad, up_mat, contract_cols, preferred_element_typ...  4.34 us
    dot_general x1, matrix products, expert_grads(): lax.dot_general(active, rows_cot, contract_rows, preferred_element_type=j...  3.55 us

profile of v2, /device:TPU:0, one launch (start us, length us, event | category | flops | bytes accessed | tf_op | source)
XLA Modules:
  0.0 174.3 jit_solution(11685526082762077678)
XLA Ops:
  0.7 1.4 fusion.24
  2.8 0.8 slice_bitcast_fusion.3
  3.5 0.8 slice_bitcast_fusion.2
  4.3 0.9 fusion.51
  7.1 0.7 convert_element_type.97
  7.8 0.7 convert_element_type.99
  8.6 1.8 %fusion.17 = f32[128,4,64]{0,2,1:T(8,128)} fusion(f32[1,4,64,64]{3,2,1,0:T(8,128)} %param.30, f32[128,64]{0,1:T(8,128)S(1)} %convert_element_type.97, f32[128,4]{0,1:T(4,128)S(1)} %get-tuple-element.45), kind=kOutput, calls=%fused_computation.41 | convolution fusion | flops 25198592 | bytes 231424 | tf_op jit(solution)/shard_map/thn,hpn->thp/dot_general | solution.py:80
  10.4 0.9 copy.39
  11.3 1.6 copy.38
  12.9 1.3 convolution_multiply_fusion.1
  14.3 1.0 fusion.26.a_ref
  15.2 51.5 %gather_rows.1 = (bf16[1024,2048]{1,0:T(8,128)(2,1)}, bf16[1024,2048]{1,0:T(8,128)(2,1)}, f32[8,8,128]{2,1,0:T(8,128)}) custom-call(bf16[128,2048]{1,0:T(8,128)(2,1)} %fusion.26.a_ref, bf16[128,2048]{1,0:T(8,128)(2,1)} %b_ref.1, f32[8,128]{1,0:T(8,128)} %pad_maximum_fusion.w_ref), custom_call_target="tpu_custom_call" | custom-call | tf_op jit(solution)/shard_map/gather_rows/pallas_call | solution.py:360
  66.8 0.8 constant_dynamic-slice_fusion.1
  67.6 0.8 slice.25
  69.2 4.4 %fusion.5 = f32[1024,448]{0,1:T(8,128)S(1)} fusion(bf16[1024,2048]{1,0:T(8,128)(2,1)} %get-tuple-element.16, bf16[1,2048,448]{1,2,0:T(8,128)(2,1)S(1)} %copy-done), kind=kOutput, calls=%fused_computation.11 | convolution fusion | flops 1879048192 | bytes 7864320 | tf_op jit(solution)/shard_map/dot_general | solution.py:147
  73.7 2.1 %fusion.8 = f32[1024,448]{0,1:T(8,128)S(1)} fusion(bf16[1024,2048]{1,0:T(8,128)(2,1)S(1)} %copy-done.22, bf16[1,2048,448]{1,2,0:T(8,128)(2,1)S(1)} %copy-done.25), kind=kOutput, calls=%fused_computation.14 | convolution fusion | flops 1879048192 | bytes 7864320 | tf_op jit(solution)/shard_map/dot_general | solution.py:148
  75.9 3.6 %fusion = bf16[1,448,2048]{2,1,0:T(8,128)(2,1)} fusion(bf16[1024,2048]{1,0:T(8,128)(2,1)S(1)} %copy-done.23, f32[1024]{0:T(1024)S(1)} %bitcast.123, f32[1024,448]{0,1:T(8,128)S(1)} %fusion.8, f32[1024,448]{0,1:T(8,128)S(1)} %fusion.5), kind=kOutput, calls=%fused_computation.5 | convolution fusion | flops 1889009664 | bytes 9703424 | tf_op jit(solution)/shard_map/dot_general | solution.py:151
  79.4 2.7 %multiply_convert_fusion.2 = (bf16[1024,448]{0,1:T(8,128)(2,1)S(1)}, bf16[1024,448]{0,1:T(8,128)(2,1)S(1)}) fusion(f32[1024,448]{0,1:T(8,128)S(1)} %fusion.5, f32[1024,448]{0,1:T(8,128)S(1)} %fusion.8, bf16[1,448,2048]{2,1,0:T(8,128)(2,1)S(1)} %copy-done.24, bf16[1024,2048]{1,0:T(8,128)(2,1)S(1)} %copy-done.23, f32[1024]{0:T(1024)S(1)} %bitcast.124), kind=kOutput, calls=%fused_computation.19 | convolution fusion | flops 1891303424 | bytes 11538432 | tf_op jit(solution)/shard_map/dot_general | solution.py:152
  82.1 3.5 %fusion.2 = bf16[1,2048,448]{1,2,0:T(8,128)(2,1)} fusion(bf16[1024,448]{0,1:T(8,128)(2,1)S(1)} %get-tuple-element.39, bf16[1024,2048]{1,0:T(8,128)(2,1)S(1)} %copy-done.22), kind=kOutput, calls=%fused_computation.7 | convolution fusion | flops 1879965696 | bytes 6946816 | tf_op jit(solution)/shard_map/dot_general | solution.py:162
  85.6 3.3 %fusion.1 = bf16[1,2048,448]{1,2,0:T(8,128)(2,1)} fusion(bf16[1024,448]{0,1:T(8,128)(2,1)S(1)} %get-tuple-element.40, bf16[1024,2048]{1,0:T(8,128)(2,1)S(1)} %copy-done.22), kind=kOutput, calls=%fused_computation.6 | convolution fusion | flops 1879965696 | bytes 6946816 | tf_op jit(solution)/shard_map/dot_general | solution.py:159
  88.9 2.4 %fusion.3 = f32[1024,2048]{1,0:T(8,128)S(1)} fusion(bf16[1024,448]{0,1:T(8,128)(2,1)S(1)} %get-tuple-element.40, bf16[1,2048,448]{1,2,0:T(8,128)(2,1)S(1)} %copy-done), kind=kOutput, calls=%fused_computation.9 | convolution fusion | flops 1879048192 | bytes 11141120 | tf_op jit(solution)/shard_map/dot_general | solution.py:165
  91.3 4.3 %add_convert_fusion.p_ref = bf16[1024,2048]{1,0:T(8,128)(2,1)} fusion(f32[1024,2048]{1,0:T(8,128)S(1)} %fusion.3, bf16[1024,448]{0,1:T(8,128)(2,1)S(1)} %get-tuple-element.39, bf16[1,2048,448]{1,2,0:T(8,128)(2,1)S(1)} %copy-done.25), kind=kOutput, calls=%fused_computation | convolution fusion | flops 1883242496 | bytes 15335424 | tf_op jit(solution)/shard_map/dot_general | solution.py:168
  95.6 39.0 %total_rows.1 = bf16[128,2048]{1,0:T(8,128)(2,1)} custom-call(bf16[1024,2048]{1,0:T(8,128)(2,1)} %add_convert_fusion.p_ref), custom_call_target="tpu_custom_call" | custom-call | tf_op jit(solution)/shard_map/total_rows/pallas_call | solution.py:501
  134.7 1.4 fusion.27
  136.1 1.5 fusion.29
  139.5 0.7 copy.43
  142.4 1.2 fusion.23
  143.6 1.4 convolution_convert_fusion.3.p_ref
  145.1 24.8 %carry_and_total.1 = (f32[128,128]{1,0:T(8,128)}, f32[256,256]{1,0:T(8,128)}) custom-call(f32[7,4]{1,0:T(8,128)} %concatenate.11.coef_ref, bf16[128,128]{1,0:T(8,128)(2,1)} %reshape.112.carry_ref, bf16[2048,256]{1,0:T(8,128)(2,1)} %convolution_convert_fusion.3.p_ref), custom_call_target="tpu_custom_call" | custom-call | tf_op jit(solution)/shard_map/carry_and_total/pallas_call | solution.py:610
  169.9 1.0 reshape.116
  171.3 0.9 fusion.22
  172.9 0.7 copy.42
  (79 shorter events, 9.2 us)
Async XLA Ops:
  0.6 68.5 %copy-start = (bf16[1,2048,448]{1,2,0:T(8,128)(2,1)S(1)}, bf16[1,2048,448]{1,2,0:T(8,128)(2,1)}, u32[]{:S(2)}) copy-start(bf16[1,2048,448]{1,2,0:T(8,128)(2,1)} %param.21) | copy-start | bytes 5505028
  0.7 13.6 %copy-start.1 = (bf16[128,2048]{1,0:T(8,128)(2,1)S(1)}, bf16[128,2048]{1,0:T(8,128)(2,1)}, u32[]{:S(2)}) copy-start(bf16[128,2048]{1,0:T(8,128)(2,1)} %param.16) | copy-start | bytes 1572868
  0.7 13.6 %copy-start.14 = (f32[2048]{0:T(1024)S(1)}, f32[2048]{0:T(1024)}, u32[]{:S(2)}) copy-start(f32[2048]{0:T(1024)} %param.17) | copy-start | bytes 24580
  2.1 64.7 %copy-start.21 = (f32[128]{0:T(128)}, f32[128]{0:T(128)S(1)}, u32[]{:S(2)}) copy-start(f32[128]{0:T(128)S(1)} %add_rsqrt_fusion) | copy-start | bytes 1540
  7.1 66.5 %copy-start.18 = (f32[128,4]{0,1:T(4,128)}, f32[128,4]{0,1:T(4,128)S(1)}, u32[]{:S(2)}) copy-start(f32[128,4]{0,1:T(4,128)S(1)} %get-tuple-element.45) | copy-start | bytes 6148
  7.1 66.5 %copy-start.15 = (pred[128,128]{1,0:T(8,128)(4,1)}, pred[128,128]{1,0:T(8,128)(4,1)S(1)}, u32[]{:S(2)}) copy-start(pred[128,128]{1,0:T(8,128)(4,1)S(1)} %iota_compare_fusion) | copy-start | bytes 49156
  7.8 65.8 %copy-start.7 = (f32[128,64]{0,1:T(8,128)}, f32[128,64]{0,1:T(8,128)S(1)}, u32[]{:S(2)}) copy-start(f32[128,64]{0,1:T(8,128)S(1)} %convert_element_type.97) | copy-start | bytes 98308
  8.6 65.1 %copy-start.11 = (f32[128,64]{0,1:T(8,128)}, f32[128,64]{0,1:T(8,128)S(1)}, u32[]{:S(2)}) copy-start(f32[128,64]{0,1:T(8,128)S(1)} %convert_element_type.99) | copy-start | bytes 98308
  69.2 4.5 %copy-start.22 = (bf16[1024,2048]{1,0:T(8,128)(2,1)S(1)}, bf16[1024,2048]{1,0:T(8,128)(2,1)}, u32[]{:S(2)}) copy-start(bf16[1024,2048]{1,0:T(8,128)(2,1)} %get-tuple-element.16) | copy-start | bytes 12582916
  69.2 4.5 %copy-start.25 = (bf16[1,2048,448]{1,2,0:T(8,128)(2,1)S(1)}, bf16[1,2048,448]{1,2,0:T(8,128)(2,1)}, u32[]{:S(2)}) copy-start(bf16[1,2048,448]{1,2,0:T(8,128)(2,1)} %param.22) | copy-start | bytes 5505028
  73.7 2.2 %copy-start.23 = (bf16[1024,2048]{1,0:T(8,128)(2,1)S(1)}, bf16[1024,2048]{1,0:T(8,128)(2,1)}, u32[]{:S(2)}) copy-start(bf16[1024,2048]{1,0:T(8,128)(2,1)} %get-tuple-element.15) | copy-start | bytes 12582916
  75.9 3.6 %copy-start.24 = (bf16[1,448,2048]{2,1,0:T(8,128)(2,1)S(1)}, bf16[1,448,2048]{2,1,0:T(8,128)(2,1)}, u32[]{:S(2)}) copy-start(bf16[1,448,2048]{2,1,0:T(8,128)(2,1)} %param.23) | copy-start | bytes 5505028
  95.6 40.5 %copy-start.2 = (bf16[128,2048]{1,0:T(8,128)(2,1)S(1)}, bf16[128,2048]{1,0:T(8,128)(2,1)}, u32[]{:S(2)}) copy-start(bf16[128,2048]{1,0:T(8,128)(2,1)} %b_ref.1) | copy-start | bytes 1572868
  134.7 3.7 %copy-start.3 = (bf16[2048,256]{1,0:T(8,128)(2,1)S(1)}, bf16[2048,256]{1,0:T(8,128)(2,1)}, u32[]{:S(2)}) copy-start(bf16[2048,256]{1,0:T(8,128)(2,1)} %param.31) | copy-start | bytes 3145732
  136.1 2.8 %copy-start.4 = (f32[4,128,128]{2,1,0:T(8,128)S(1)}, f32[4,128,128]{2,1,0:T(8,128)}, u32[]{:S(2)}) copy-start(f32[4,128,128]{2,1,0:T(8,128)} %convolution_multiply_fusion.1) | copy-start | bytes 786436
  136.1 2.8 %copy-start.9 = (f32[128,4,64]{0,2,1:T(8,128)S(1)}, f32[128,4,64]{0,2,1:T(8,128)}, u32[]{:S(2)}) copy-start(f32[128,4,64]{0,2,1:T(8,128)} %fusion.17) | copy-start | bytes 393220
  136.1 2.8 %copy-start.10 = (f32[128,256]{0,1:T(8,128)S(1)}, f32[128,256]{0,1:T(8,128)}, u32[]{:S(2)}) copy-start(f32[128,256]{0,1:T(8,128)} %copy.38) | copy-start | bytes 393220
  136.1 2.8 %copy-start.17 = (f32[4,128]{1,0:T(4,128)S(1)}, f32[4,128]{1,0:T(4,128)}, u32[]{:S(2)}) copy-start(f32[4,128]{1,0:T(4,128)} %param.26) | copy-start | bytes 6148
  137.6 2.7 %copy-start.8 = (f32[128,64]{0,1:T(8,128)S(1)}, f32[128,64]{0,1:T(8,128)}, u32[]{:S(2)}) copy-start(f32[128,64]{0,1:T(8,128)} %copy-done.7) | copy-start | bytes 98308
  137.6 2.7 %copy-start.19 = (f32[128,4]{0,1:T(4,128)S(1)}, f32[128,4]{0,1:T(4,128)}, u32[]{:S(2)}) copy-start(f32[128,4]{0,1:T(4,128)} %copy-done.18) | copy-start | bytes 6148
  137.7 3.7 %copy-start.6 = (f32[1,4,64,64]{3,2,1,0:T(8,128)S(1)}, f32[1,4,64,64]{3,2,1,0:T(8,128)}, u32[]{:S(2)}) copy-start(f32[1,4,64,64]{3,2,1,0:T(8,128)} %param.30) | copy-start | bytes 196612
  138.3 3.4 %copy-start.16 = (pred[128,128]{1,0:T(8,128)(4,1)S(1)}, pred[128,128]{1,0:T(8,128)(4,1)}, u32[]{:S(2)}) copy-start(pred[128,128]{1,0:T(8,128)(4,1)} %copy-done.15) | copy-start | bytes 49156
  138.3 4.1 %copy-start.12 = (f32[128,64]{0,1:T(8,128)S(1)}, f32[128,64]{0,1:T(8,128)}, u32[]{:S(2)}) copy-start(f32[128,64]{0,1:T(8,128)} %copy-done.11) | copy-start | bytes 98308
  141.8 29.1 %copy-start.20 = (f32[128,4]{0,1:T(4,128)S(1)}, f32[128,4]{0,1:T(4,128)}, u32[]{:S(2)}) copy-start(f32[128,4]{0,1:T(4,128)} %get-tuple-element.44) | copy-start | bytes 6148
  143.6 28.9 %copy-start.5 = (f32[4,128,128]{2,1,0:T(8,128)S(1)}, f32[4,128,128]{2,1,0:T(8,128)}, u32[]{:S(2)}) copy-start(f32[4,128,128]{2,1,0:T(8,128)} %convolution_multiply_fusion.1) | copy-start | bytes 786436
  169.9 3.7 %copy-start.13 = (f32[256,256]{1,0:T(8,128)S(1)}, f32[256,256]{1,0:T(8,128)}, u32[]{:S(2)}) copy-start(f32[256,256]{1,0:T(8,128)} %get-tuple-element.63) | copy-start | bytes 786436

commit v3 on v2

--- a/solution.py
+++ b/solution.py
@@ -409,66 +409,59 @@
         copy = core_copy(i)
         copy.start()
         made.append(copy)
-    firsts, seconds = [], []
-    for i in range(nz):
+    firsts, seconds, along = [], [], []
+
+    def first(i):
         made[i].wait_recv()
         at = lanes(plane(i), 2 * rows)
         s1[at] = (p_ref[at, lanes(c, half)].astype(f32) + rc[at].astype(f32)).astype(bf16)
+        sems = (m_sem.at[0, i], m_sem.at[1, i])
         if i % 2 == 0:
-            copy = remote(
-                s1.at[at, lanes(1 - y, quarter)],
-                ra.at[i // 2],
-                m_sem.at[0, i],
-                m_sem.at[1, i],
-                over_y,
-            )
+            copy = remote(s1.at[at, lanes(1 - y, quarter)], ra.at[i // 2], *sems, over_y)
         else:
-            copy = remote(
-                s1.at[lanes(plane(i) * 2 + 1 - x, rows)],
-                rb.at[i // 2],
-                m_sem.at[0, i],
-                m_sem.at[1, i],
-                over_x,
-            )
+            block = lanes(plane(i) * 2 + 1 - x, rows)
+            copy = remote(s1.at[block], rb.at[i // 2], *sems, over_x)
         copy.start()
         firsts.append(copy)
-    for i in range(nz):
+
+    def second(i):
         firsts[i].wait_recv()
         k = i // 2
+        sems = (n_sem.at[0, i], n_sem.at[1, i])
         if i % 2 == 0:
             at = lanes(plane(i), 2 * rows)
             sa[k] = (s1[at, lanes(y, quarter)].astype(f32) + ra[k].astype(f32)).astype(bf16)
-            copy = remote(
-                sa.at[k, lanes(1 - x, rows)], r2.at[i], n_sem.at[0, i], n_sem.at[1, i], over_x
-            )
+            copy = remote(sa.at[k, lanes(1 - x, rows)], r2.at[i], *sems, over_x)
         else:
             at = lanes(plane(i) * 2 + x, rows)
             sb[k] = (s1[at].astype(f32) + rb[k].astype(f32)).astype(bf16)
-            copy = remote(
-                sb.at[k, :, lanes(1 - y, quarter)],
-                r2.at[i],
-                n_sem.at[0, i],
-                n_sem.at[1, i],
-                over_y,
-            )
+            copy = remote(sb.at[k, :, lanes(1 - y, quarter)], r2.at[i], *sems, over_y)
         copy.start()
         seconds.append(copy)
-    along = []
-    total = None
-    for i in range(nz):
+
+    def third(i):
         seconds[i].wait_recv()
         k = i // 2
         held = sa[k, lanes(x, rows)] if i % 2 == 0 else sb[k, :, lanes(y, quarter)]
         value = held.astype(f32) + r2[i].astype(f32)
         if i < nz - 1:
             s3[i] = value.astype(bf16)
-            copy = remote(
-                s3.at[i], rz.at[i], z_sem.at[0, i], z_sem.at[1, i], (plane(i) * 2 + x, tp)
-            )
+            target = (plane(i) * 2 + x, tp)
+            copy = remote(s3.at[i], rz.at[i], z_sem.at[0, i], z_sem.at[1, i], target)
             copy.start()
             along.append(copy)
-        else:
-            total = value
+        return value
+
+    lead = min(3, nz)
+    for i in range(lead):
+        first(i)
+    for i in range(nz):
+        second(i)
+        if i + lead < nz:
+            first(i + lead)
+        if i > 0:
+            third(i - 1)
+    total = third(nz - 1)
     for i in range(nz - 1):
         along[i].wait_recv()
         total = total + rz[i].astype(f32)

time: 175 us -> 173 us (0.989)
  Pallas kernels: 115 us -> 113 us
    pallas_call x1, Pallas kernels: 39 us -> 37.1 us  [total_rows(): pl.pallas_call(functools.partial(total_kernel, nz), out_shape=jax.ShapeDt...]
where the time goes in v3:
time: 173 us; the launch traced here: 172 us
  Pallas kernels  113 us (65%)
  matrix products  36.5 us (21%)
  local copies, waits for them, and re-layouts  11.4 us (7%)
  other arithmetic  9.94 us (6%)
    pallas_call x1, Pallas kernels, gather_rows(): pl.pallas_call(functools.partial(gather_kernel, nz), out_shape=(whole, wh...  51.5 us
    pallas_call x1, Pallas kernels, total_rows(): pl.pallas_call(functools.partial(total_kernel, nz), out_shape=jax.ShapeDt...  37.1 us
    pallas_call x1, Pallas kernels, carry_and_total(): pl.pallas_call(functools.partial(carry_kernel, nz), out_shape=(jax.ShapeD...  24.4 us
    dot_general x1, matrix products, expert_grads(): gate_pre = jnp.dot(rows_in, gate_mat, preferred_element_type=jnp.float32)  4.43 us
    dot_general x1, matrix products, expert_grads(): lax.dot_general(up_pre_grad, up_mat, contract_cols, preferred_element_typ...  4.34 us
    dot_general x1, matrix products, expert_grads(): lax.dot_general(active, rows_cot, contract_rows, preferred_element_type=j...  3.55 us
    dot_general x1, matrix products, expert_grads(): lax.dot_general(rows_in, up_pre_grad, contract_rows, preferred_element_ty...  3.49 us

profile of v3, /device:TPU:0, one launch (start us, length us, event | category | flops | bytes accessed | tf_op | source)
XLA Modules:
  0.0 171.9 jit_solution(10142410837241029487)
XLA Ops:
  0.7 1.4 fusion.24
  2.8 0.8 slice_bitcast_fusion.3
  3.5 0.8 slice_bitcast_fusion.2
  4.3 0.9 fusion.51
  7.1 0.7 convert_element_type.97
  7.8 0.7 convert_element_type.99
  8.6 1.8 %fusion.17 = f32[128,4,64]{0,2,1:T(8,128)} fusion(f32[1,4,64,64]{3,2,1,0:T(8,128)} %param.30, f32[128,64]{0,1:T(8,128)S(1)} %convert_element_type.97, f32[128,4]{0,1:T(4,128)S(1)} %get-tuple-element.45), kind=kOutput, calls=%fused_computation.41 | convolution fusion | flops 25198592 | bytes 231424 | tf_op jit(solution)/shard_map/thn,hpn->thp/dot_general | solution.py:80
  10.4 0.9 copy.39
  11.3 1.6 copy.38
  12.9 1.3 convolution_multiply_fusion.1
  14.3 1.0 fusion.26.a_ref
  15.2 51.5 %gather_rows.1 = (bf16[1024,2048]{1,0:T(8,128)(2,1)}, bf16[1024,2048]{1,0:T(8,128)(2,1)}, f32[8,8,128]{2,1,0:T(8,128)}) custom-call(bf16[128,2048]{1,0:T(8,128)(2,1)} %fusion.26.a_ref, bf16[128,2048]{1,0:T(8,128)(2,1)} %b_ref.1, f32[8,128]{1,0:T(8,128)} %pad_maximum_fusion.w_ref), custom_call_target="tpu_custom_call" | custom-call | tf_op jit(solution)/shard_map/gather_rows/pallas_call | solution.py:360
  66.8 0.8 constant_dynamic-slice_fusion.1
  67.6 0.8 slice.25
  69.2 4.4 %fusion.5 = f32[1024,448]{0,1:T(8,128)S(1)} fusion(bf16[1024,2048]{1,0:T(8,128)(2,1)} %get-tuple-element.16, bf16[1,2048,448]{1,2,0:T(8,128)(2,1)S(1)} %copy-done), kind=kOutput, calls=%fused_computation.11 | convolution fusion | flops 1879048192 | bytes 7864320 | tf_op jit(solution)/shard_map/dot_general | solution.py:147
  73.7 2.1 %fusion.8 = f32[1024,448]{0,1:T(8,128)S(1)} fusion(bf16[1024,2048]{1,0:T(8,128)(2,1)S(1)} %copy-done.22, bf16[1,2048,448]{1,2,0:T(8,128)(2,1)S(1)} %copy-done.25), kind=kOutput, calls=%fused_computation.14 | convolution fusion | flops 1879048192 | bytes 7864320 | tf_op jit(solution)/shard_map/dot_general | solution.py:148
  75.9 3.6 %fusion = bf16[1,448,2048]{2,1,0:T(8,128)(2,1)} fusion(bf16[1024,2048]{1,0:T(8,128)(2,1)S(1)} %copy-done.23, f32[1024]{0:T(1024)S(1)} %bitcast.123, f32[1024,448]{0,1:T(8,128)S(1)} %fusion.8, f32[1024,448]{0,1:T(8,128)S(1)} %fusion.5), kind=kOutput, calls=%fused_computation.5 | convolution fusion | flops 1889009664 | bytes 9703424 | tf_op jit(solution)/shard_map/dot_general | solution.py:151
  79.4 2.7 %multiply_convert_fusion.2 = (bf16[1024,448]{0,1:T(8,128)(2,1)S(1)}, bf16[1024,448]{0,1:T(8,128)(2,1)S(1)}) fusion(f32[1024,448]{0,1:T(8,128)S(1)} %fusion.5, f32[1024,448]{0,1:T(8,128)S(1)} %fusion.8, bf16[1,448,2048]{2,1,0:T(8,128)(2,1)S(1)} %copy-done.24, bf16[1024,2048]{1,0:T(8,128)(2,1)S(1)} %copy-done.23, f32[1024]{0:T(1024)S(1)} %bitcast.124), kind=kOutput, calls=%fused_computation.19 | convolution fusion | flops 1891303424 | bytes 11538432 | tf_op jit(solution)/shard_map/dot_general | solution.py:152
  82.1 3.5 %fusion.2 = bf16[1,2048,448]{1,2,0:T(8,128)(2,1)} fusion(bf16[1024,448]{0,1:T(8,128)(2,1)S(1)} %get-tuple-element.39, bf16[1024,2048]{1,0:T(8,128)(2,1)S(1)} %copy-done.22), kind=kOutput, calls=%fused_computation.7 | convolution fusion | flops 1879965696 | bytes 6946816 | tf_op jit(solution)/shard_map/dot_general | solution.py:162
  85.6 3.3 %fusion.1 = bf16[1,2048,448]{1,2,0:T(8,128)(2,1)} fusion(bf16[1024,448]{0,1:T(8,128)(2,1)S(1)} %get-tuple-element.40, bf16[1024,2048]{1,0:T(8,128)(2,1)S(1)} %copy-done.22), kind=kOutput, calls=%fused_computation.6 | convolution fusion | flops 1879965696 | bytes 6946816 | tf_op jit(solution)/shard_map/dot_general | solution.py:159
  88.9 2.4 %fusion.3 = f32[1024,2048]{1,0:T(8,128)S(1)} fusion(bf16[1024,448]{0,1:T(8,128)(2,1)S(1)} %get-tuple-element.40, bf16[1,2048,448]{1,2,0:T(8,128)(2,1)S(1)} %copy-done), kind=kOutput, calls=%fused_computation.9 | convolution fusion | flops 1879048192 | bytes 11141120 | tf_op jit(solution)/shard_map/dot_general | solution.py:165
  91.3 4.3 %add_convert_fusion.p_ref = bf16[1024,2048]{1,0:T(8,128)(2,1)} fusion(f32[1024,2048]{1,0:T(8,128)S(1)} %fusion.3, bf16[1024,448]{0,1:T(8,128)(2,1)S(1)} %get-tuple-element.39, bf16[1,2048,448]{1,2,0:T(8,128)(2,1)S(1)} %copy-done.25), kind=kOutput, calls=%fused_computation | convolution fusion | flops 1883242496 | bytes 15335424 | tf_op jit(solution)/shard_map/dot_general | solution.py:168
  95.6 37.1 %total_rows.1 = bf16[128,2048]{1,0:T(8,128)(2,1)} custom-call(bf16[1024,2048]{1,0:T(8,128)(2,1)} %add_convert_fusion.p_ref), custom_call_target="tpu_custom_call" | custom-call | tf_op jit(solution)/shard_map/total_rows/pallas_call | solution.py:494
  132.7 1.4 fusion.27
  134.1 1.5 fusion.29
  137.6 0.7 copy.43
  140.4 1.2 fusion.23
  141.6 1.4 convolution_convert_fusion.3.p_ref
  143.1 24.4 %carry_and_total.1 = (f32[128,128]{1,0:T(8,128)}, f32[256,256]{1,0:T(8,128)}) custom-call(f32[7,4]{1,0:T(8,128)} %concatenate.11.coef_ref, bf16[128,128]{1,0:T(8,128)(2,1)} %reshape.112.carry_ref, bf16[2048,256]{1,0:T(8,128)(2,1)} %convolution_convert_fusion.3.p_ref), custom_call_target="tpu_custom_call" | custom-call | tf_op jit(solution)/shard_map/carry_and_total/pallas_call | solution.py:603
  167.5 1.0 reshape.116
  168.8 0.9 fusion.22
  170.4 0.7 copy.42
  (79 shorter events, 9.2 us)
Async XLA Ops:
  0.6 68.5 %copy-start = (bf16[1,2048,448]{1,2,0:T(8,128)(2,1)S(1)}, bf16[1,2048,448]{1,2,0:T(8,128)(2,1)}, u32[]{:S(2)}) copy-start(bf16[1,2048,448]{1,2,0:T(8,128)(2,1)} %param.21) | copy-start | bytes 5505028
  0.7 13.6 %copy-start.1 = (bf16[128,2048]{1,0:T(8,128)(2,1)S(1)}, bf16[128,2048]{1,0:T(8,128)(2,1)}, u32[]{:S(2)}) copy-start(bf16[128,2048]{1,0:T(8,128)(2,1)} %param.16) | copy-start | bytes 1572868
  0.7 13.6 %copy-start.14 = (f32[2048]{0:T(1024)S(1)}, f32[2048]{0:T(1024)}, u32[]{:S(2)}) copy-start(f32[2048]{0:T(1024)} %param.17) | copy-start | bytes 24580
  2.1 64.7 %copy-start.21 = (f32[128]{0:T(128)}, f32[128]{0:T(128)S(1)}, u32[]{:S(2)}) copy-start(f32[128]{0:T(128)S(1)} %add_rsqrt_fusion) | copy-start | bytes 1540
  7.1 66.5 %copy-start.18 = (f32[128,4]{0,1:T(4,128)}, f32[128,4]{0,1:T(4,128)S(1)}, u32[]{:S(2)}) copy-start(f32[128,4]{0,1:T(4,128)S(1)} %get-tuple-element.45) | copy-start | bytes 6148
  7.1 66.5 %copy-start.15 = (pred[128,128]{1,0:T(8,128)(4,1)}, pred[128,128]{1,0:T(8,128)(4,1)S(1)}, u32[]{:S(2)}) copy-start(pred[128,128]{1,0:T(8,128)(4,1)S(1)} %iota_compare_fusion) | copy-start | bytes 49156
  7.8 65.8 %copy-start.7 = (f32[128,64]{0,1:T(8,128)}, f32[128,64]{0,1:T(8,128)S(1)}, u32[]{:S(2)}) copy-start(f32[128,64]{0,1:T(8,128)S(1)} %convert_element_type.97) | copy-start | bytes 98308
  8.6 65.1 %copy-start.11 = (f32[128,64]{0,1:T(8,128)}, f32[128,64]{0,1:T(8,128)S(1)}, u32[]{:S(2)}) copy-start(f32[128,64]{0,1:T(8,128)S(1)} %convert_element_type.99) | copy-start | bytes 98308
  69.2 4.5 %copy-start.22 = (bf16[1024,2048]{1,0:T(8,128)(2,1)S(1)}, bf16[1024,2048]{1,0:T(8,128)(2,1)}, u32[]{:S(2)}) copy-start(bf16[1024,2048]{1,0:T(8,128)(2,1)} %get-tuple-element.16) | copy-start | bytes 12582916
  69.2 4.5 %copy-start.25 = (bf16[1,2048,448]{1,2,0:T(8,128)(2,1)S(1)}, bf16[1,2048,448]{1,2,0:T(8,128)(2,1)}, u32[]{:S(2)}) copy-start(bf16[1,2048,448]{1,2,0:T(8,128)(2,1)} %param.22) | copy-start | bytes 5505028
  73.7 2.2 %copy-start.23 = (bf16[1024,2048]{1,0:T(8,128)(2,1)S(1)}, bf16[1024,2048]{1,0:T(8,128)(2,1)}, u32[]{:S(2)}) copy-start(bf16[1024,2048]{1,0:T(8,128)(2,1)} %get-tuple-element.15) | copy-start | bytes 12582916
  75.9 3.6 %copy-start.24 = (bf16[1,448,2048]{2,1,0:T(8,128)(2,1)S(1)}, bf16[1,448,2048]{2,1,0:T(8,128)(2,1)}, u32[]{:S(2)}) copy-start(bf16[1,448,2048]{2,1,0:T(8,128)(2,1)} %param.23) | copy-start | bytes 5505028
  95.6 38.5 %copy-start.2 = (bf16[128,2048]{1,0:T(8,128)(2,1)S(1)}, bf16[128,2048]{1,0:T(8,128)(2,1)}, u32[]{:S(2)}) copy-start(bf16[128,2048]{1,0:T(8,128)(2,1)} %b_ref.1) | copy-start | bytes 1572868
  132.7 3.7 %copy-start.3 = (bf16[2048,256]{1,0:T(8,128)(2,1)S(1)}, bf16[2048,256]{1,0:T(8,128)(2,1)}, u32[]{:S(2)}) copy-start(bf16[2048,256]{1,0:T(8,128)(2,1)} %param.31) | copy-start | bytes 3145732
  134.1 2.8 %copy-start.4 = (f32[4,128,128]{2,1,0:T(8,128)S(1)}, f32[4,128,128]{2,1,0:T(8,128)}, u32[]{:S(2)}) copy-start(f32[4,128,128]{2,1,0:T(8,128)} %convolution_multiply_fusion.1) | copy-start | bytes 786436
  134.1 2.8 %copy-start.9 = (f32[128,4,64]{0,2,1:T(8,128)S(1)}, f32[128,4,64]{0,2,1:T(8,128)}, u32[]{:S(2)}) copy-start(f32[128,4,64]{0,2,1:T(8,128)} %fusion.17) | copy-start | bytes 393220
  134.1 2.8 %copy-start.10 = (f32[128,256]{0,1:T(8,128)S(1)}, f32[128,256]{0,1:T(8,128)}, u32[]{:S(2)}) copy-start(f32[128,256]{0,1:T(8,128)} %copy.38) | copy-start | bytes 393220
  134.1 2.8 %copy-start.17 = (f32[4,128]{1,0:T(4,128)S(1)}, f32[4,128]{1,0:T(4,128)}, u32[]{:S(2)}) copy-start(f32[4,128]{1,0:T(4,128)} %param.26) | copy-start | bytes 6148
  135.6 2.7 %copy-start.8 = (f32[128,64]{0,1:T(8,128)S(1)}, f32[128,64]{0,1:T(8,128)}, u32[]{:S(2)}) copy-start(f32[128,64]{0,1:T(8,128)} %copy-done.7) | copy-start | bytes 98308
  135.7 2.7 %copy-start.19 = (f32[128,4]{0,1:T(4,128)S(1)}, f32[128,4]{0,1:T(4,128)}, u32[]{:S(2)}) copy-start(f32[128,4]{0,1:T(4,128)} %copy-done.18) | copy-start | bytes 6148
  135.7 3.7 %copy-start.6 = (f32[1,4,64,64]{3,2,1,0:T(8,128)S(1)}, f32[1,4,64,64]{3,2,1,0:T(8,128)}, u32[]{:S(2)}) copy-start(f32[1,4,64,64]{3,2,1,0:T(8,128)} %param.30) | copy-start | bytes 196612
  136.4 3.4 %copy-start.16 = (pred[128,128]{1,0:T(8,128)(4,1)S(1)}, pred[128,128]{1,0:T(8,128)(4,1)}, u32[]{:S(2)}) copy-start(pred[128,128]{1,0:T(8,128)(4,1)} %copy-done.15) | copy-start | bytes 49156
  136.4 4.1 %copy-start.12 = (f32[128,64]{0,1:T(8,128)S(1)}, f32[128,64]{0,1:T(8,128)}, u32[]{:S(2)}) copy-start(f32[128,64]{0,1:T(8,128)} %copy-done.11) | copy-start | bytes 98308
  139.8 28.7 %copy-start.20 = (f32[128,4]{0,1:T(4,128)S(1)}, f32[128,4]{0,1:T(4,128)}, u32[]{:S(2)}) copy-start(f32[128,4]{0,1:T(4,128)} %get-tuple-element.44) | copy-start | bytes 6148
  141.6 28.4 %copy-start.5 = (f32[4,128,128]{2,1,0:T(8,128)S(1)}, f32[4,128,128]{2,1,0:T(8,128)}, u32[]{:S(2)}) copy-start(f32[4,128,128]{2,1,0:T(8,128)} %convolution_multiply_fusion.1) | copy-start | bytes 786436
  167.4 3.7 %copy-start.13 = (f32[256,256]{1,0:T(8,128)S(1)}, f32[256,256]{1,0:T(8,128)}, u32[]{:S(2)}) copy-start(f32[256,256]{1,0:T(8,128)} %get-tuple-element.63) | copy-start | bytes 786436
